TPU v7x, 256 devices: a whole 4x4x8 slice. The times are simulated.
256 devices in a mesh: ep: 64 (over z, x, core), tp: 4 (over y).
Axes of the slice: x: 4, y: 4, z: 8, core: 2. Of those that a mesh axis runs over, the one named last changes fastest.
Arguments:
- query_rows: bfloat16 [16384, 1024], P('ep', 'tp'), may hold values from -8 to 8
- key_rows: bfloat16 [16384, 256], P('ep', 'tp'), may hold values from -8 to 8
- value_rows: bfloat16 [16384, 256], P('ep', 'tp'), may hold values from -16 to 16
- query_gain: float32 [64], replicated, may hold values from 0.5 to 7.5
- key_gain: float32 [64], replicated, may hold values from 0.5 to 7.5
- moe_tokens: bfloat16 [32768, 2048], P(('ep', 'tp')), may hold values from -6 to 6
- norm_gain: float32 [2048], replicated, may hold values from 0.1 to 1.9
- routes: int32 [32768, 2], P('ep'), may hold values from 0 to 63, all different within a row; in each aligned block of 128 rows (0 to 127, 128 to 255, ...) at most 8 rows name the same one
- route_weights: float32 [32768, 2], P('ep'), may hold values from 0.1 to 1
- expert_gate: bfloat16 [64, 2048, 1024], P('ep', None, 'tp'), may hold values from -0.125 to 0.125
- expert_up: bfloat16 [64, 2048, 1024], P('ep', None, 'tp'), may hold values from -0.125 to 0.125
- expert_down: bfloat16 [64, 1024, 2048], P('ep', 'tp'), may hold values from -0.1875 to 0.1875
- shared_gate: bfloat16 [2048, 1024], P(None, 'tp'), may hold values from -0.125 to 0.125
- shared_up: bfloat16 [2048, 1024], P(None, 'tp'), may hold values from -0.125 to 0.125
- shared_down: bfloat16 [1024, 2048], P('tp'), may hold values from -0.1875 to 0.1875
Outputs:
- attn_out: bfloat16 [16384, 1024], P('ep', 'tp')
- moe_out: bfloat16 [32768, 2048], P(('ep', 'tp'))
Inputs may be any that keep to these rules, and one draw needn't show every extreme that they name: `routes`: each row names 2 different experts. Within each aligned block of 128 rows no expert is named more than 8 times, and in every draw some expert is named exactly 8 times in some block.
All inputs are finite; a program needn't handle non-finite values.
Results may differ from a plain program's by a relative error of at most 0.012.
The roundings to bfloat16 on the way count: a program that leaves them out, or rounds other values in their place, can miss the bound.
Values may be sent and summed in bfloat16 or wider, within the bound.
A program may use at most 192 MiB of HBM per device.

v0:
```python
import jax
import jax.numpy as jnp
from jax import lax
from jax.sharding import Mesh
from jax.sharding import PartitionSpec as P

GRID_W = 64
EP = ("ep_0", "ep_1", "ep_2")
EP_TP = ("ep_0", "ep_1", "ep_2", "tp")


epsilon = 1e-06
rotary_base = 10000.0
routed_scale = 2.5


def joined_along(pieces, dim):
    lengths = list(pieces.shape[1:])
    lengths[dim] *= pieces.shape[0]
    return jnp.moveaxis(pieces, 0, dim).reshape(lengths)


def stacked_from(array, axes, order):
    pieces = array
    for k in order:
        pieces = lax.all_gather(pieces, axes[k])
    done = order[::-1]
    back = [done.index(k) for k in range(len(axes))]
    pieces = pieces.transpose(*back, *range(len(axes), pieces.ndim))
    return pieces.reshape(-1, *array.shape)


def gathered_by_axis(array, axes, order, dim):
    return joined_along(stacked_from(array, axes, order), dim)


def copy_for_each(array, axis):
    count = lax.axis_size(axis)
    return lax.all_to_all(
        jnp.broadcast_to(array[None], (count, *array.shape)), axis, 0, 0, tiled=True
    )


def gathered_copies(array, axis, dim):
    pieces = copy_for_each(array, axis)
    return joined_along(pieces, dim)


def cut_along(array, dim, count):
    before, after = (array.shape[:dim], array.shape[dim + 1 :])
    return jnp.moveaxis(array.reshape(*before, count, -1, *after), dim, 0)


def sent_and_summed(array, axis, dim):
    pieces = cut_along(array, dim, lax.axis_size(axis))
    arrived = lax.all_to_all(pieces, axis, split_axis=0, concat_axis=0, tiled=True)
    return arrived.astype(jnp.float32).sum(axis=0)


def rotate_heads(heads_in, gain_row, positions):
    values32 = heads_in.astype(jnp.float32)
    scaled = (
        values32
        * lax.rsqrt(jnp.mean(values32 * values32, axis=-1, keepdims=True) + epsilon)
        * gain_row
    )
    pair_count = scaled.shape[-1] // 4
    inv_freq = rotary_base ** (-jnp.arange(pair_count, dtype=jnp.float32) / pair_count)
    grid_row = (positions // GRID_W).astype(jnp.float32)
    grid_col = (positions % GRID_W).astype(jnp.float32)
    angles = jnp.concatenate([grid_row[:, None] * inv_freq, grid_col[:, None] * inv_freq], axis=-1)[
        :, None, :
    ]
    cosine = jnp.cos(angles)
    sine_part = jnp.sin(angles)
    first_half = scaled[..., 0::2]
    second_half = scaled[..., 1::2]
    turned = jnp.stack(
        [
            first_half * cosine - second_half * sine_part,
            first_half * sine_part + second_half * cosine,
        ],
        axis=-1,
    )
    return turned.reshape(scaled.shape).astype(jnp.bfloat16)


def span_length(row_count):
    length = min(row_count, 2048)
    while row_count % length:
        length -= 1
    return length


def attend(query_rows, key_rows, value_rows, query_gain, key_gain):
    row_count = query_rows.shape[0]
    head_size = query_gain.shape[0]
    q_heads = query_rows.shape[1] // head_size
    kv_heads = key_rows.shape[1] // head_size
    group = q_heads // kv_heads
    scale = head_size ** (-0.5)
    positions = lax.axis_index(EP) * row_count + jnp.arange(row_count, dtype=jnp.int32)
    q_rot = rotate_heads(query_rows.reshape(row_count, q_heads, head_size), query_gain, positions)
    k_rot = rotate_heads(key_rows.reshape(row_count, kv_heads, head_size), key_gain, positions)
    key_value = jnp.stack([k_rot, value_rows.reshape(row_count, kv_heads, head_size)], axis=2)
    key_value = key_value.reshape(row_count, kv_heads * 2 * head_size)
    q_grouped = q_rot.reshape(row_count, kv_heads, group, head_size).transpose(1, 2, 0, 3)
    q_grouped = q_grouped.reshape(kv_heads, group * row_count, head_size)
    query_count = group * row_count
    initial = (
        jnp.full((kv_heads, query_count), -jnp.inf, jnp.float32),
        jnp.zeros((kv_heads, query_count), jnp.float32),
        jnp.zeros((kv_heads, query_count, head_size), jnp.float32),
    )

    def one_span(carried, span_rows):
        run_max, run_sum, mixed = carried
        keys_span = span_rows[:, :, 0, :]
        values_span = span_rows[:, :, 1, :]
        scores = (
            jnp.einsum("hrd,shd->hrs", q_grouped, keys_span, preferred_element_type=jnp.float32)
            * scale
        )
        new_max = jnp.maximum(run_max, jnp.max(scores, axis=-1))
        factor = jnp.exp(run_max - new_max)
        weights = jnp.exp(scores - new_max[..., None])
        run_sum = run_sum * factor + jnp.sum(weights, axis=-1)
        added = jnp.einsum(
            "hrs,shd->hrd",
            weights.astype(jnp.bfloat16),
            values_span,
            preferred_element_type=jnp.float32,
        )
        mixed = mixed * factor[..., None] + added
        return ((new_max, run_sum, mixed), None)

    carried = initial
    piece_rows = gathered_by_axis(key_value, (("ep_0", "ep_1"), "ep_2"), (0, 1), 0)
    piece_count = piece_rows.shape[0]
    length = span_length(piece_count)
    spans = piece_rows.reshape(piece_count // length, length, kv_heads, 2, head_size)
    carried, unused = lax.scan(one_span, carried, spans)
    run_max, run_sum, mixed = carried
    result = (mixed / run_sum[..., None]).astype(jnp.bfloat16)
    result = result.reshape(kv_heads, group, row_count, head_size).transpose(2, 0, 1, 3)
    return result.reshape(row_count, q_heads * head_size)


def slot_ranks(route_rows, tok_rows, experts):
    top_count = route_rows.shape[1]
    blocks = route_rows.shape[0] // tok_rows
    chosen = route_rows.reshape(blocks, tok_rows * top_count)
    one_hot = (chosen[:, :, None] == jnp.arange(experts, dtype=jnp.int32)[None, None, :]).astype(
        jnp.int32
    )
    ranks = jnp.sum((jnp.cumsum(one_hot, axis=1) - one_hot) * one_hot, axis=2)
    return (chosen, ranks)


def build_send(source, chosen, ranks, tok_rows, top_count, capacity, experts):
    blocks = chosen.shape[0]
    model_width = source.shape[1]
    block_ids = jnp.arange(blocks, dtype=jnp.int32)[:, None]
    dest = (chosen * blocks + block_ids) * capacity + ranks
    rows_from = (
        block_ids * tok_rows
        + jnp.arange(tok_rows * top_count, dtype=jnp.int32)[None, :] // top_count
    )
    slot_rows = jnp.full((experts * blocks * capacity,), blocks * tok_rows, jnp.int32)
    slot_rows = slot_rows.at[dest.reshape(-1)].set(rows_from.reshape(-1))
    padded = jnp.concatenate([source, jnp.zeros((1, model_width), source.dtype)], axis=0)
    return padded[slot_rows].reshape(experts, blocks * capacity, model_width)


def expert_products(arrived, w_gate, w_up, w_down):
    gate_proj = jnp.einsum("lrd,ldf->lrf", arrived, w_gate, preferred_element_type=jnp.float32)
    up_proj = jnp.einsum("lrd,ldf->lrf", arrived, w_up, preferred_element_type=jnp.float32)
    hidden = (jax.nn.silu(gate_proj) * up_proj).astype(jnp.bfloat16)
    return jnp.einsum("lrf,lfd->lrd", hidden, w_down, preferred_element_type=jnp.float32)


def shared_products(rows_in, w_gate, w_up, w_down):
    gate_proj = jnp.dot(rows_in, w_gate, preferred_element_type=jnp.float32)
    up_proj = jnp.dot(rows_in, w_up, preferred_element_type=jnp.float32)
    hidden = (jax.nn.silu(gate_proj) * up_proj).astype(jnp.bfloat16)
    return jnp.dot(hidden, w_down, preferred_element_type=jnp.float32)


def experts_half(
    moe_tokens,
    norm_gain,
    routes,
    route_weights,
    expert_gate,
    expert_up,
    expert_down,
    shared_gate,
    shared_up,
    shared_down,
):
    tok_rows, model_width = moe_tokens.shape
    top_count = routes.shape[1]
    tp_size = lax.axis_size("tp")
    ep_size = lax.axis_size(EP)
    local_experts = expert_gate.shape[0]
    experts = local_experts * ep_size
    capacity = 2 * tok_rows * top_count // experts
    lane = lax.axis_index("tp")
    values32 = moe_tokens.astype(jnp.float32)
    normed = (
        values32
        * lax.rsqrt(jnp.mean(values32 * values32, axis=-1, keepdims=True) + epsilon)
        * norm_gain
    ).astype(jnp.bfloat16)
    gates = route_weights / jnp.sum(route_weights, axis=-1, keepdims=True) * routed_scale
    own_gates = lax.dynamic_slice_in_dim(gates, lane * tok_rows, tok_rows, 0)
    group_rows = gathered_copies(normed.reshape(1, 1, 1, tok_rows, model_width), "tp", 2)
    chosen, ranks = slot_ranks(routes, tok_rows, experts)
    send = build_send(
        group_rows.reshape(tp_size * tok_rows, model_width),
        chosen,
        ranks,
        tok_rows,
        top_count,
        capacity,
        experts,
    )
    arrived = lax.all_to_all(send, EP, split_axis=0, concat_axis=1, tiled=True)
    own_chosen = lax.dynamic_index_in_dim(chosen, lane, 0, keepdims=False)
    own_ranks = lax.dynamic_index_in_dim(ranks, lane, 0, keepdims=False)
    routed_part = expert_products(arrived, expert_gate, expert_up, expert_down)
    shared_part = shared_products(
        group_rows.reshape(tp_size * tok_rows, model_width), shared_gate, shared_up, shared_down
    )
    routed_sum, shared_sum = (
        sent_and_summed(
            routed_part.reshape(local_experts, ep_size, tp_size, capacity, model_width).astype(
                jnp.bfloat16
            ),
            "tp",
            2,
        ),
        sent_and_summed(
            shared_part.reshape(1, 1, tp_size, tok_rows, model_width).astype(jnp.bfloat16), "tp", 2
        ),
    )
    outgoing = routed_sum.astype(jnp.bfloat16).reshape(
        local_experts, ep_size * capacity, model_width
    )
    returned = lax.all_to_all(outgoing, EP, split_axis=1, concat_axis=0, tiled=True)
    flat_rows = returned.reshape(experts * capacity, model_width)
    picked = flat_rows[own_chosen * capacity + own_ranks].reshape(tok_rows, top_count, model_width)
    routed_total = jnp.sum(own_gates[:, :, None] * picked.astype(jnp.float32), axis=1)
    return (routed_total + shared_sum.reshape(tok_rows, model_width)).astype(jnp.bfloat16)


def body(
    query_rows,
    key_rows,
    value_rows,
    query_gain,
    key_gain,
    moe_tokens,
    norm_gain,
    routes,
    route_weights,
    expert_gate,
    expert_up,
    expert_down,
    shared_gate,
    shared_up,
    shared_down,
):
    attn_out = attend(query_rows, key_rows, value_rows, query_gain, key_gain)
    moe_out = experts_half(
        moe_tokens,
        norm_gain,
        routes,
        route_weights,
        expert_gate,
        expert_up,
        expert_down,
        shared_gate,
        shared_up,
        shared_down,
    )
    return (attn_out, moe_out)


def solution(mesh):
    finer = Mesh(mesh.devices.reshape(8, 4, 2, mesh.shape["tp"]), ("ep_0", "ep_1", "ep_2", "tp"))
    return jax.shard_map(
        body,
        mesh=finer,
        in_specs=(
            P(EP, "tp"),
            P(EP, "tp"),
            P(EP, "tp"),
            P(),
            P(),
            P(EP_TP, None),
            P(),
            P(EP, None),
            P(EP, None),
            P(EP, None, "tp"),
            P(EP, None, "tp"),
            P(EP, "tp", None),
            P(None, "tp"),
            P(None, "tp"),
            P("tp", None),
        ),
        out_specs=(P(EP, "tp"), P(EP_TP, None)),
        check_vma=False,
    )
```

profile of v0, /device:TPU:8, one launch (start us, length us, event | category | flops | bytes accessed | tf_op | source)
XLA Modules:
  0.0 509.0 jit_solution(16651082673510238095)
XLA Ops:
  11.4 5.7 %all-to-all-start = ((bf16[4,1,1,1,128,2048]{5,4,3,2,1,0:T(8,128)(2,1)}), bf16[4,1,1,1,128,2048]{5,4,3,2,1,0:T(8,128)(2,1)S(1)}, u32[]{:S(2)}, u32[]{:S(2)}) async-start(bf16[4,1,1,1,128,2048]{5,4,3,2,1,0:T(8,128)(2,1)} %broadcast_in_dim.15), calls=%async_computation | async-start | bytes 4194304 | tf_op jit(solution)/shard_map/all_to_all | solution.py:39
  18.8 4.5 reduce-window.6
  25.4 4.3 scatter_custom_fusion
  29.8 11.4 %all-to-all-done = bf16[4,1,1,1,128,2048]{5,4,3,2,1,0:T(8,128)(2,1)S(1)} async-done(((bf16[4,1,1,1,128,2048]{5,4,3,2,1,0:T(8,128)(2,1)}), bf16[4,1,1,1,128,2048]{5,4,3,2,1,0:T(8,128)(2,1)S(1)}, u32[]{:S(2)}, u32[]{:S(2)}) %all-to-all-start) | async-done | bytes 2097184 | tf_op jit(solution)/shard_map/all_to_all | solution.py:39
  44.3 11.0 %gather_fusion = bf16[2048,2048]{1,0:T(8,128)(2,1)} fusion(bf16[513,2048]{1,0:T(8,128)(2,1)S(1)} %concatenate.33, s32[2048]{0:T(1024)S(1)} %fusion.48), kind=kCustom, calls=%fused_computation | custom fusion | bytes 16785408 | tf_op jit(solution)/shard_map/gather | solution.py:172
  55.3 12.3 %all-to-all-start.1 = ((bf16[64,32,2048]{2,1,0:T(8,128)(2,1)}), bf16[64,32,2048]{2,1,0:T(8,128)(2,1)}, u32[]{:S(2)}, u32[]{:S(2)}) async-start(bf16[64,32,2048]{2,1,0:T(8,128)(2,1)} %bitcast.157), calls=%async_computation.1 | async-start | bytes 16777216 | tf_op jit(solution)/shard_map/all_to_all | solution.py:228
  69.0 2.7 fusion.60
  71.7 5.4 %convolution_convert_fusion = bf16[512,2048]{1,0:T(8,128)(2,1)} fusion(bf16[256,2048]{1,0:T(8,128)(2,1)} %param.31, bf16[512,2048]{1,0:T(8,128)(2,1)S(1)} %bitcast.163, bf16[2048,256]{1,0:T(8,128)(2,1)} %param.30, f32[512,256]{1,0:T(8,128)} %fusion.60), kind=kOutput, calls=%fused_computation.25 | convolution fusion | flops 1075576832 | bytes 6815744 | tf_op jit(solution)/shard_map/dot_general | solution.py:186
  77.1 189.0 %all-to-all-done.1 = bf16[64,32,2048]{2,1,0:T(8,128)(2,1)} async-done(((bf16[64,32,2048]{2,1,0:T(8,128)(2,1)}), bf16[64,32,2048]{2,1,0:T(8,128)(2,1)}, u32[]{:S(2)}, u32[]{:S(2)}) %all-to-all-start.1) | async-done | bytes 8388640 | tf_op jit(solution)/shard_map/all_to_all | solution.py:228
  266.1 5.1 %all-to-all-start.4 = ((bf16[4,1,1,1,128,2048]{5,4,3,2,1,0:T(8,128)(2,1)}), bf16[4,1,1,1,128,2048]{5,4,3,2,1,0:T(8,128)(2,1)S(1)}, u32[]{:S(2)}, u32[]{:S(2)}) async-start(bf16[4,1,1,1,128,2048]{5,4,3,2,1,0:T(8,128)(2,1)} %bitcast.168), calls=%async_computation.4 | async-start | bytes 4194304 | tf_op jit(solution)/shard_map/all_to_all | solution.py:56
  271.3 6.0 %fusion.23 = f32[2048,256]{1,0:T(8,128)S(1)} fusion(bf16[2048,2048]{1,0:T(8,128)(2,1)} %bitcast.24, bf16[1,2048,256]{2,1,0:T(8,128)(2,1)} %param.26), kind=kOutput, calls=%fused_computation.39 | convolution fusion | flops 2147483648 | bytes 11534336 | tf_op jit(solution)/shard_map/lrd,ldf->lrf/dot_general | solution.py:176
  277.3 6.0 %fusion.16 = bf16[2048,256]{1,0:T(8,128)(2,1)S(1)} fusion(bf16[2048,2048]{1,0:T(8,128)(2,1)} %bitcast.24, f32[2048,256]{1,0:T(8,128)S(1)} %fusion.23, bf16[1,2048,256]{2,1,0:T(8,128)(2,1)S(1)} %copy-done.11), kind=kOutput, calls=%fused_computation.27 | convolution fusion | flops 2150629376 | bytes 12582912 | tf_op jit(solution)/shard_map/lrd,ldf->lrf/dot_general | solution.py:177
  283.3 5.5 %convert_bitcast_fusion = bf16[4,1,64,1,8,2048]{5,4,0,2,3,1:T(8,128)(2,1)} fusion(bf16[64,4,8,256]{3,2,1,0:T(8,128)(2,1)S(1)} %bitcast.169, bf16[1,256,2048]{2,1,0:T(8,128)(2,1)S(1)} %copy-done), kind=kOutput, calls=%fused_computation.23 | convolution fusion | flops 2151677952 | bytes 10485760 | tf_op jit(solution)/shard_map/lrf,lfd->lrd/dot_general | solution.py:179
  288.9 8.3 %copy.87 = bf16[4,1,64,1,8,2048]{5,4,2,3,1,0:T(8,128)(2,1)} copy(bf16[4,1,64,1,8,2048]{5,4,0,2,3,1:T(8,128)(2,1)} %convert_bitcast_fusion) | data formatting | bytes 16777216 | tf_op jit(solution)/shard_map/transpose | solution.py:51
  297.2 5.8 %all-to-all-start.2 = ((bf16[4,1,64,1,8,2048]{5,4,2,3,1,0:T(8,128)(2,1)}), bf16[4,1,64,1,8,2048]{5,4,2,3,1,0:T(8,128)(2,1)}, u32[]{:S(2)}, u32[]{:S(2)}) async-start(bf16[4,1,64,1,8,2048]{5,4,2,3,1,0:T(8,128)(2,1)} %copy.87), calls=%async_computation.2 | async-start | bytes 16777216 | tf_op jit(solution)/shard_map/all_to_all | solution.py:56
  306.4 15.9 %all-gather.6.cloned.1.call-done = bf16[64,256,128]{2,1,0:T(8,128)(2,1)} async-done(((bf16[32,256,128]{2,1,0:T(8,128)(2,1)}), bf16[64,256,128]{2,1,0:T(8,128)(2,1)}) %all-gather.6.cloned.1.call-update) | async-done | bytes 4194320 | tf_op jit(solution)/shard_map/all_gather | solution.py:26
  322.3 11.5 %copy.74 = bf16[32,2,256,128]{2,1,0,3:T(2,128)(2,1)} copy(bf16[32,2,256,128]{3,2,0,1:T(8,128)(2,1)} %bitcast.165) | data formatting | bytes 8388608 | tf_op jit(solution)/shard_map/transpose | solution.py:29
  333.7 7.9 %reshape_reshape_reshape.3 = bf16[8,2048,1,2,64]{1,0,4,3,2:T(8,128)(2,1)} reshape(bf16[32,2,256,128]{2,1,0,3:T(2,128)(2,1)} %copy.74) | data formatting | bytes 8388608 | tf_op jit(solution)/shard_map/reshape;reshape;reshape | solution.py:141
  341.6 6.4 %copy.77 = bf16[8,2048,1,2,64]{1,4,3,2,0:T(8,128)(2,1)} copy(bf16[8,2048,1,2,64]{1,0,4,3,2:T(8,128)(2,1)} %reshape_reshape_reshape.3) | data formatting | bytes 8388608
  348.0 43.8 %all-to-all-done.2 = bf16[4,1,64,1,8,2048]{5,4,2,3,1,0:T(8,128)(2,1)} async-done(((bf16[4,1,64,1,8,2048]{5,4,2,3,1,0:T(8,128)(2,1)}), bf16[4,1,64,1,8,2048]{5,4,2,3,1,0:T(8,128)(2,1)}, u32[]{:S(2)}, u32[]{:S(2)}) %all-to-all-start.2) | async-done | bytes 8388640 | tf_op jit(solution)/shard_map/all_to_all | solution.py:56
  391.8 5.7 %reduce_sum.94 = bf16[64,8,2048]{2,1,0:T(8,128)(2,1)S(1)} reduce(bf16[4,1,64,1,8,2048]{5,4,2,3,1,0:T(8,128)(2,1)} %all-to-all-done.2, bf16[]{:T(256)} %constant.138.clone.1), dimensions={0,1,3}, to_apply=%region_12.13 | reduce | flops 3145728 | bytes 10485762 | tf_op jit(solution)/shard_map/reduce_sum | solution.py:57
  397.5 5.2 %copy.102 = bf16[1,512,2048]{2,0,1:T(2,128)(2,1)} copy(bf16[1,512,2048]{2,1,0:T(8,128)(2,1)S(1)} %bitcast.164) | data formatting | bytes 4194304 | tf_op jit(solution)/shard_map/reshape | solution.py:247
  403.2 13.2 %reduce.11 = bf16[512,2048]{1,0:T(8,128)(2,1)S(1)} reduce(bf16[512,1,2048]{2,1,0:T(2,128)(2,1)} %bitcast.158, bf16[]{:T(256)} %broadcast.392), dimensions={1}, to_apply=%bitcast.136.reduce_sub_computation | reduce | bytes 4194306
  416.3 3.3 reshape.559
  419.6 10.7 %all-to-all-start.3 = ((bf16[64,2,8192]{2,1,0:T(2,128)(2,1)}), bf16[64,2,8192]{2,1,0:T(2,128)(2,1)S(1)}, u32[]{:S(2)}, u32[]{:S(2)}) async-start(bf16[64,2,8192]{2,1,0:T(2,128)(2,1)} %reshape.559), calls=%async_computation.3 | async-start | bytes 4194304 | tf_op jit(solution)/shard_map/all_to_all | solution.py:250
  430.3 43.8 %while.15 = (s32[]{:T(128)}, f32[1,1024]{1,0:T(1,128)S(1)}, f32[1,1024]{1,0:T(1,128)S(1)}, f32[1,1024,64]{1,2,0:T(8,128)S(1)}, bf16[8,2048,1,2,64]{1,4,3,2,0:T(8...) while((s32[]{:T(128)}, f32[1,1024]{1,0:T(1,128)S(1)}, ...), condition=%wide.region_5.6_spmd.clone, body=%wide.region_2.5_spmd.clone.sunk | while | flops 553849856 | bytes 27590764 | solution.py:142
  475.0 6.4 %all-to-all-done.3 = bf16[64,2,8192]{2,1,0:T(2,128)(2,1)S(1)} async-done(((bf16[64,2,8192]{2,1,0:T(2,128)(2,1)}), bf16[64,2,8192]{2,1,0:T(2,128)(2,1)S(1)}, u32[]{:S(2)}, u32[]{:S(2)}) %all-to-all-start.3) | async-done | bytes 2097184 | tf_op jit(solution)/shard_map/all_to_all | solution.py:250
  481.4 6.8 %reshape.560 = bf16[512,1,2048]{2,1,0:T(2,128)(2,1)} reshape(bf16[64,2,8192]{2,1,0:T(2,128)(2,1)S(1)} %all-to-all-done.3) | data formatting | bytes 4194304
  488.2 3.5 copy.101
  491.6 2.3 gather_fusion.1
  494.0 2.4 reshape.526
  496.4 3.2 multiply_reduce_fusion.1
  (154 shorter events, 62.5 us)
Async XLA Ops:
  7.2 276.2 %copy-start = (bf16[1,256,2048]{2,1,0:T(8,128)(2,1)S(1)}, bf16[1,256,2048]{2,1,0:T(8,128)(2,1)}, u32[]{:S(2)}) copy-start(bf16[1,256,2048]{2,1,0:T(8,128)(2,1)} %param.28) | copy-start | bytes 3145732
  7.2 9.9 %copy-start.7 = (s32[512,2]{0,1:T(2,128)S(1)}, s32[512,2]{0,1:T(2,128)}, u32[]{:S(2)}) copy-start(s32[512,2]{0,1:T(2,128)} %param.24) | copy-start | bytes 12292
  11.4 29.8 %all-to-all-start = ((bf16[4,1,1,1,128,2048]{5,4,3,2,1,0:T(8,128)(2,1)}), bf16[4,1,1,1,128,2048]{5,4,3,2,1,0:T(8,128)(2,1)S(1)}, u32[]{:S(2)}, u32[]{:S(2)}) async-start(bf16[4,1,1,1,128,2048]{5,4,3,2,1,0:T(8,128)(2,1)} %broadcast_in_dim.15), calls=%async_computation | async-start | bytes 4194304 | tf_op jit(solution)/shard_map/all_to_all | solution.py:39
  41.2 1.4 copy-start.2
  55.3 12.4 %copy-start.4 = (bf16[256,64]{0,1:T(8,128)(2,1)S(1)}, bf16[256,64]{0,1:T(8,128)(2,1)}, u32[]{:S(2)}) copy-start(bf16[256,64]{0,1:T(8,128)(2,1)} %param.18) | copy-start | bytes 98308
  55.3 12.5 %copy-start.9 = (f32[64]{0:T(128)S(1)}, f32[64]{0:T(128)}, u32[]{:S(2)}) copy-start(f32[64]{0:T(128)} %param.21) | copy-start | bytes 772
  55.3 12.9 %copy-start.6 = (bf16[256,64]{0,1:T(8,128)(2,1)S(1)}, bf16[256,64]{0,1:T(8,128)(2,1)}, u32[]{:S(2)}) copy-start(bf16[256,64]{0,1:T(8,128)(2,1)} %param.19) | copy-start | bytes 98308
  55.3 13.7 %copy-start.3 = (bf16[4,1,1,1,128,2048]{5,4,3,2,1,0:T(8,128)(2,1)S(1)}, bf16[4,1,1,1,128,2048]{5,4,3,2,1,0:T(8,128)(2,1)}, u32[]{:S(2)}) copy-start(bf16[4,1,1,1,128,2048]{5,4,3,2,1,0:T(8,128)(2,1)} %copy-done.2) | copy-start | bytes 6291460
  55.3 210.8 %all-to-all-start.1 = ((bf16[64,32,2048]{2,1,0:T(8,128)(2,1)}), bf16[64,32,2048]{2,1,0:T(8,128)(2,1)}, u32[]{:S(2)}, u32[]{:S(2)}) async-start(bf16[64,32,2048]{2,1,0:T(8,128)(2,1)} %bitcast.157), calls=%async_computation.1 | async-start | bytes 16777216 | tf_op jit(solution)/shard_map/all_to_all | solution.py:228
  67.7 235.4 %all-gather.4.cloned.1.call-start = ((), (), s32[]{:S(2)}) async-start(), calls=%async_computation.5 | async-start | bytes 2162688 | tf_op jit(solution)/shard_map/all_gather | solution.py:26
  266.1 31.1 %all-to-all-start.4 = ((bf16[4,1,1,1,128,2048]{5,4,3,2,1,0:T(8,128)(2,1)}), bf16[4,1,1,1,128,2048]{5,4,3,2,1,0:T(8,128)(2,1)S(1)}, u32[]{:S(2)}, u32[]{:S(2)}) async-start(bf16[4,1,1,1,128,2048]{5,4,3,2,1,0:T(8,128)(2,1)} %bitcast.168), calls=%async_computation.4 | async-start | bytes 4194304 | tf_op jit(solution)/shard_map/all_to_all | solution.py:56
  271.2 6.1 %copy-start.11 = (bf16[1,2048,256]{2,1,0:T(8,128)(2,1)S(1)}, bf16[1,2048,256]{2,1,0:T(8,128)(2,1)}, u32[]{:S(2)}) copy-start(bf16[1,2048,256]{2,1,0:T(8,128)(2,1)} %param.27) | copy-start | bytes 3145732
  297.2 6.6 %copy-start.5 = (bf16[256,256]{1,0:T(8,128)(2,1)S(1)}, bf16[256,256]{1,0:T(8,128)(2,1)}, u32[]{:S(2)}) copy-start(bf16[256,256]{1,0:T(8,128)(2,1)} %param.17) | copy-start | bytes 393220
  297.2 6.8 %copy-start.10 = (f32[64]{0:T(128)S(1)}, f32[64]{0:T(128)}, u32[]{:S(2)}) copy-start(f32[64]{0:T(128)} %param.20) | copy-start | bytes 772
  297.2 7.0 %copy-start.8 = (f32[512,2]{0,1:T(2,128)S(1)}, f32[512,2]{0,1:T(2,128)}, u32[]{:S(2)}) copy-start(f32[512,2]{0,1:T(2,128)} %param.25) | copy-start | bytes 12292
  297.2 94.6 %all-to-all-start.2 = ((bf16[4,1,64,1,8,2048]{5,4,2,3,1,0:T(8,128)(2,1)}), bf16[4,1,64,1,8,2048]{5,4,2,3,1,0:T(8,128)(2,1)}, u32[]{:S(2)}, u32[]{:S(2)}) async-start(bf16[4,1,64,1,8,2048]{5,4,2,3,1,0:T(8,128)(2,1)} %copy.87), calls=%async_computation.2 | async-start | bytes 16777216 | tf_op jit(solution)/shard_map/all_to_all | solution.py:56
  303.0 19.3 %all-gather.6.cloned.1.call-start = ((), (), s32[]{:S(2)}) async-start(), calls=%async_computation.6 | async-start | bytes 6291456 | tf_op jit(solution)/shard_map/all_gather | solution.py:26
  419.6 61.8 %all-to-all-start.3 = ((bf16[64,2,8192]{2,1,0:T(2,128)(2,1)}), bf16[64,2,8192]{2,1,0:T(2,128)(2,1)S(1)}, u32[]{:S(2)}, u32[]{:S(2)}) async-start(bf16[64,2,8192]{2,1,0:T(2,128)(2,1)} %reshape.559), calls=%async_computation.3 | async-start | bytes 4194304 | tf_op jit(solution)/shard_map/all_to_all | solution.py:250
  491.6 10.1 %copy-start.1 = (bf16[1,256,2048]{2,1,0:T(8,128)(2,1)S(1)}, bf16[1,256,2048]{2,1,0:T(8,128)(2,1)}, u32[]{:S(2)}) copy-start(bf16[1,256,2048]{2,1,0:T(8,128)(2,1)} %param.28) | copy-start | bytes 3145732
Sparse Core Ops, SparseCore 0:
  71.6 107.7 all-gather.3
  305.6 16.6 all-gather.5
where the time goes:
time: 518 us; the launch traced here: 509 us
  waiting for transfers between devices  267 us (52%)
  local copies, waits for them, and re-layouts  91.8 us (18%)
  matrix products  48.7 us (9%)
  other arithmetic  46.1 us (9%)
  starting transfers between devices  39.7 us (8%)
  between operations  15 us (3%)
    all_to_all x1, waiting for transfers between devices, experts_half(): arrived = lax.all_to_all(send, EP, split_axis=0, concat_axis=1, tiled=True)  189 us
    all_to_all x2, waiting for transfers between devices, sent_and_summed(): lax.all_to_all(pieces, axis, split_axis=0, concat_axis=0, tiled=True)  43.8 us
    unnamed x37, local copies, waits for them, and re-layouts  23.1 us
    all_gather x2, waiting for transfers between devices, stacked_from(): pieces = lax.all_gather(pieces, axes[k])  15.9 us
    unnamed x5, other arithmetic  13.2 us
    dot_general x8, matrix products, one_span(): jnp.einsum('hrs,shd->hrd', weights.astype(jnp.bfloat16), values_span, pre...  12.5 us
    all_to_all x1, starting transfers between devices, experts_half(): arrived = lax.all_to_all(send, EP, split_axis=0, concat_axis=1, tiled=True)  12.3 us
    transpose x1, local copies, waits for them, and re-layouts, stacked_from(): pieces = pieces.transpose(*back, *range(len(axes), pieces.ndim))  11.5 us
  transfers between devices with their start and end apart: 7, of which 5 were waited for; matrix products, arithmetic and copies ran while one was open for 24% of the time, Pallas kernels for 0%

commit v1 on v0

--- a/solution.py
+++ b/solution.py
@@ -146,44 +146,41 @@
     return result.reshape(row_count, q_heads * head_size)
 
 
-def slot_ranks(route_rows, tok_rows, experts):
-    top_count = route_rows.shape[1]
-    blocks = route_rows.shape[0] // tok_rows
-    chosen = route_rows.reshape(blocks, tok_rows * top_count)
-    one_hot = (chosen[:, :, None] == jnp.arange(experts, dtype=jnp.int32)[None, None, :]).astype(
-        jnp.int32
-    )
-    ranks = jnp.sum((jnp.cumsum(one_hot, axis=1) - one_hot) * one_hot, axis=2)
-    return (chosen, ranks)
-
-
-def build_send(source, chosen, ranks, tok_rows, top_count, capacity, experts):
-    blocks = chosen.shape[0]
-    model_width = source.shape[1]
-    block_ids = jnp.arange(blocks, dtype=jnp.int32)[:, None]
-    dest = (chosen * blocks + block_ids) * capacity + ranks
-    rows_from = (
-        block_ids * tok_rows
-        + jnp.arange(tok_rows * top_count, dtype=jnp.int32)[None, :] // top_count
-    )
-    slot_rows = jnp.full((experts * blocks * capacity,), blocks * tok_rows, jnp.int32)
-    slot_rows = slot_rows.at[dest.reshape(-1)].set(rows_from.reshape(-1))
-    padded = jnp.concatenate([source, jnp.zeros((1, model_width), source.dtype)], axis=0)
-    return padded[slot_rows].reshape(experts, blocks * capacity, model_width)
-
-
-def expert_products(arrived, w_gate, w_up, w_down):
-    gate_proj = jnp.einsum("lrd,ldf->lrf", arrived, w_gate, preferred_element_type=jnp.float32)
-    up_proj = jnp.einsum("lrd,ldf->lrf", arrived, w_up, preferred_element_type=jnp.float32)
-    hidden = (jax.nn.silu(gate_proj) * up_proj).astype(jnp.bfloat16)
-    return jnp.einsum("lrf,lfd->lrd", hidden, w_down, preferred_element_type=jnp.float32)
-
-
-def shared_products(rows_in, w_gate, w_up, w_down):
+def ring(step):
+    return [(i, (i + step) % 4) for i in range(4)]
+
+
+def token_slots(own_routes, capacity):
+    rows = own_routes.shape[0]
+    earlier = jnp.arange(rows)[:, None] < jnp.arange(rows)[None, :]
+    slots = []
+    for k in range(own_routes.shape[1]):
+        mine = own_routes[:, k]
+        same = own_routes[:, 0][:, None] == mine[None, :]
+        for other in range(1, own_routes.shape[1]):
+            same = same | (own_routes[:, other][:, None] == mine[None, :])
+        rank = jnp.sum((same & earlier).astype(jnp.int32), axis=0)
+        slots.append(mine * capacity + rank)
+    return slots
+
+
+def from_ring(array):
+    half = array.shape[0] // 2
+    left = lax.ppermute(array, "tp", ring(1))
+    right = lax.ppermute(array, "tp", ring(3))
+    far = jnp.concatenate(
+        [
+            lax.ppermute(left[:half], "tp", ring(1)),
+            lax.ppermute(right[half:], "tp", ring(3)),
+        ]
+    )
+    return [array, left, right, far]
+
+
+def hidden_rows(rows_in, w_gate, w_up):
     gate_proj = jnp.dot(rows_in, w_gate, preferred_element_type=jnp.float32)
     up_proj = jnp.dot(rows_in, w_up, preferred_element_type=jnp.float32)
-    hidden = (jax.nn.silu(gate_proj) * up_proj).astype(jnp.bfloat16)
-    return jnp.dot(hidden, w_down, preferred_element_type=jnp.float32)
+    return (jax.nn.silu(gate_proj) * up_proj).astype(jnp.bfloat16)
 
 
 def experts_half(
@@ -200,10 +197,8 @@
 ):
     tok_rows, model_width = moe_tokens.shape
     top_count = routes.shape[1]
-    tp_size = lax.axis_size("tp")
     ep_size = lax.axis_size(EP)
-    local_experts = expert_gate.shape[0]
-    experts = local_experts * ep_size
+    experts = ep_size
     capacity = 2 * tok_rows * top_count // experts
     lane = lax.axis_index("tp")
     values32 = moe_tokens.astype(jnp.float32)
@@ -212,46 +207,42 @@
         * lax.rsqrt(jnp.mean(values32 * values32, axis=-1, keepdims=True) + epsilon)
         * norm_gain
     ).astype(jnp.bfloat16)
-    gates = route_weights / jnp.sum(route_weights, axis=-1, keepdims=True) * routed_scale
-    own_gates = lax.dynamic_slice_in_dim(gates, lane * tok_rows, tok_rows, 0)
-    group_rows = gathered_copies(normed.reshape(1, 1, 1, tok_rows, model_width), "tp", 2)
-    chosen, ranks = slot_ranks(routes, tok_rows, experts)
-    send = build_send(
-        group_rows.reshape(tp_size * tok_rows, model_width),
-        chosen,
-        ranks,
-        tok_rows,
-        top_count,
-        capacity,
-        experts,
-    )
-    arrived = lax.all_to_all(send, EP, split_axis=0, concat_axis=1, tiled=True)
-    own_chosen = lax.dynamic_index_in_dim(chosen, lane, 0, keepdims=False)
-    own_ranks = lax.dynamic_index_in_dim(ranks, lane, 0, keepdims=False)
-    routed_part = expert_products(arrived, expert_gate, expert_up, expert_down)
-    shared_part = shared_products(
-        group_rows.reshape(tp_size * tok_rows, model_width), shared_gate, shared_up, shared_down
-    )
-    routed_sum, shared_sum = (
-        sent_and_summed(
-            routed_part.reshape(local_experts, ep_size, tp_size, capacity, model_width).astype(
-                jnp.bfloat16
-            ),
-            "tp",
-            2,
-        ),
-        sent_and_summed(
-            shared_part.reshape(1, 1, tp_size, tok_rows, model_width).astype(jnp.bfloat16), "tp", 2
-        ),
-    )
-    outgoing = routed_sum.astype(jnp.bfloat16).reshape(
-        local_experts, ep_size * capacity, model_width
-    )
-    returned = lax.all_to_all(outgoing, EP, split_axis=1, concat_axis=0, tiled=True)
-    flat_rows = returned.reshape(experts * capacity, model_width)
-    picked = flat_rows[own_chosen * capacity + own_ranks].reshape(tok_rows, top_count, model_width)
-    routed_total = jnp.sum(own_gates[:, :, None] * picked.astype(jnp.float32), axis=1)
-    return (routed_total + shared_sum.reshape(tok_rows, model_width)).astype(jnp.bfloat16)
+    own_routes = lax.dynamic_slice_in_dim(routes, lane * tok_rows, tok_rows, 0)
+    own_weights = lax.dynamic_slice_in_dim(route_weights, lane * tok_rows, tok_rows, 0)
+    gates = own_weights / jnp.sum(own_weights, axis=-1, keepdims=True) * routed_scale
+    slots = token_slots(own_routes, capacity)
+    places = jnp.arange(experts * capacity, dtype=jnp.int32)
+    one_hots = [(places[:, None] == slot[None, :]).astype(jnp.bfloat16) for slot in slots]
+    placed = one_hots[0] + one_hots[1]
+    send = jnp.dot(placed, normed, preferred_element_type=jnp.float32).astype(jnp.bfloat16)
+    arrived = lax.all_to_all(
+        send.reshape(experts, capacity, model_width), EP, split_axis=0, concat_axis=0, tiled=True
+    ).reshape(experts * capacity, model_width)
+    gate_parts = from_ring(expert_gate[0])
+    up_parts = from_ring(expert_up[0])
+    down_parts = from_ring(expert_down[0])
+    total = None
+    for w_gate, w_up, w_down in zip(gate_parts, up_parts, down_parts):
+        hidden = hidden_rows(arrived, w_gate, w_up)
+        part = jnp.dot(hidden, w_down, preferred_element_type=jnp.float32)
+        part = part.astype(jnp.bfloat16).astype(jnp.float32)
+        total = part if total is None else total + part
+    outgoing = total.astype(jnp.bfloat16).reshape(experts, capacity, model_width)
+    returned = lax.all_to_all(outgoing, EP, split_axis=0, concat_axis=0, tiled=True)
+    returned = returned.reshape(experts * capacity, model_width)
+    group_rows = lax.all_gather(normed, "tp", axis=0, tiled=True)
+    shared_hidden = hidden_rows(group_rows, shared_gate, shared_up)
+    shared_part = jnp.dot(shared_hidden, shared_down, preferred_element_type=jnp.float32)
+    shared_part = shared_part.astype(jnp.bfloat16).reshape(4, tok_rows, model_width)
+    shared_got = lax.all_to_all(shared_part, "tp", split_axis=0, concat_axis=0, tiled=True)
+    shared_sum = jnp.sum(shared_got.astype(jnp.float32), axis=0)
+    routed_total = 0.0
+    for k in range(top_count):
+        picked = lax.dot_general(
+            one_hots[k], returned, (((0,), (0,)), ((), ())), preferred_element_type=jnp.float32
+        )
+        routed_total = routed_total + gates[:, k : k + 1] * picked
+    return (routed_total + shared_sum).astype(jnp.bfloat16)
 
 
 def body(

time: 518 us -> 336 us (0.65); the launches traced: 509 us -> 334 us
  waiting for transfers between devices: 267 us -> 124 us
  local copies, waits for them, and re-layouts: 91.8 us -> 48.8 us
  matrix products: 48.7 us -> 86.7 us
  other arithmetic: 46.1 us -> 19.3 us
    all_to_all x5 -> x3, waiting for transfers between devices: 251 us -> 46.3 us  [the longest x1 46.3 us: experts_half(): lax.all_to_all(outgoing, EP, split_axis=0, concat_axis=0, tiled=True)]
    ppermute x0 -> x12, waiting for transfers between devices: none -> 77 us  [the longest x3 71.7 us: from_ring(): left = lax.ppermute(array, 'tp', ring(1))]
    dot_general x5 -> x13, matrix products: 25.7 us -> 51.5 us  [the longest x4 25.5 us: experts_half(): part = jnp.dot(hidden, w_down, preferred_element_type=jnp.float32)]
    all_gather x2, waiting for transfers between devices: 15.9 us -> 0.02 us  [stacked_from(): pieces = lax.all_gather(pieces, axes[k])]
    gather x2 -> x0, local copies, waits for them, and re-layouts: 13.4 us -> none  [the longest x1 11 us: build_send(): return padded[slot_rows].reshape(experts, blocks * capacity, model_width)]
    unnamed x37 -> x36, local copies, waits for them, and re-layouts: 23.1 us -> 9.8 us
    unnamed x5 -> x3, other arithmetic: 13.2 us -> 0.01 us
    dot_general x8, matrix products: 12.5 us -> 24.7 us  [one_span(): jnp.einsum('hrs,shd->hrd', weights.astype(jnp.bfloat16), values_span, pre...]
  transfers between devices with their start and end apart: 7 -> 18, of which waited for: 5 -> 5; matrix products, arithmetic and copies ran while one was open for 24% -> 19% of each run, Pallas kernels for 0% -> 0%
where the time goes in v1:
time: 336 us; the launch traced here: 334 us
  waiting for transfers between devices  124 us (37%)
  matrix products  86.7 us (26%)
  local copies, waits for them, and re-layouts  48.8 us (15%)
  starting transfers between devices  40.8 us (12%)
  other arithmetic  19.3 us (6%)
  between operations  14.1 us (4%)
    ppermute x3, waiting for transfers between devices, from_ring(): left = lax.ppermute(array, 'tp', ring(1))  71.7 us
    all_to_all x1, waiting for transfers between devices, experts_half(): lax.all_to_all(outgoing, EP, split_axis=0, concat_axis=0, tiled=True)  46.3 us
    dot_general x4, matrix products, experts_half(): part = jnp.dot(hidden, w_down, preferred_element_type=jnp.float32)  25.5 us
    dot_general x8, matrix products, one_span(): jnp.einsum('hrs,shd->hrd', weights.astype(jnp.bfloat16), values_span, pre...  24.7 us
    all_to_all x1, starting transfers between devices, experts_half(): lax.all_to_all(send.reshape(experts, capacity, model_width), EP, split_ax...  12.3 us
    reduce_sum x8, other arithmetic, one_span(): run_sum = run_sum * factor + jnp.sum(weights, axis=-1)  11.5 us
    transpose x1, local copies, waits for them, and re-layouts, stacked_from(): pieces = pieces.transpose(*back, *range(len(axes), pieces.ndim))  11.3 us
    dot_general x8, matrix products, one_span(): jnp.einsum('hrd,shd->hrs', q_grouped, keys_span, preferred_element_type=j...  10.5 us
  transfers between devices with their start and end apart: 18, of which 5 were waited for; matrix products, arithmetic and copies ran while one was open for 19% of the time, Pallas kernels for 0%

profile of v1, /device:TPU:8, one launch (start us, length us, event | category | flops | bytes accessed | tf_op | source)
XLA Modules:
  0.0 334.4 jit_solution(3881254426127493340)
XLA Ops:
  10.6 2.1 fusion.16
  12.7 12.3 %all-to-all-start = ((bf16[64,8,2048]{2,1,0:T(8,128)(2,1)}), bf16[64,8,2048]{2,1,0:T(8,128)(2,1)}, u32[]{:S(2)}, u32[]{:S(2)}) async-start(bf16[64,8,2048]{2,1,0:T(8,128)(2,1)} %fusion.16), calls=%async_computation | async-start | bytes 4194304 | tf_op jit(solution)/shard_map/all_to_all | solution.py:218
  31.6 29.3 %collective-permute-done = bf16[2048,256]{1,0:T(8,128)(2,1)S(1)} collective-permute-done((bf16[2048,256]{1,0:T(8,128)(2,1)}, bf16[2048,256]{1,0:T(8,128)(2,1)S(1)}, u32[]{:S(2)}, u32[]{:S(2)}) %collective-permute-start) | collective-permute-done | bytes 1048608 | tf_op jit(solution)/shard_map/ppermute | solution.py:169
  65.9 25.7 %collective-permute-done.1 = bf16[2048,256]{1,0:T(8,128)(2,1)} collective-permute-done((bf16[2048,256]{1,0:T(8,128)(2,1)}, bf16[2048,256]{1,0:T(8,128)(2,1)}, u32[]{:S(2)}, u32[]{:S(2)}) %collective-permute-start.1) | collective-permute-done | bytes 1048608 | tf_op jit(solution)/shard_map/ppermute | solution.py:169
  97.4 16.7 %collective-permute-done.2 = bf16[256,2048]{1,0:T(8,128)(2,1)} collective-permute-done((bf16[256,2048]{1,0:T(8,128)(2,1)}, bf16[256,2048]{1,0:T(8,128)(2,1)}, u32[]{:S(2)}, u32[]{:S(2)}) %collective-permute-start.2) | collective-permute-done | bytes 1048608 | tf_op jit(solution)/shard_map/ppermute | solution.py:169
  119.9 3.5 %fusion.132 = f32[512,256]{1,0:T(8,128)} fusion(bf16[512,2048]{1,0:T(8,128)(2,1)} %all-gather.7.cloned.1.call-done, bf16[2048,256]{1,0:T(8,128)(2,1)} %param.29), kind=kOutput, calls=%fused_computation.167 | convolution fusion | flops 536870912 | bytes 3670016 | tf_op jit(solution)/shard_map/dot_general | solution.py:181
  123.4 5.0 %convolution_convert_fusion = bf16[512,2048]{1,0:T(8,128)(2,1)} fusion(bf16[256,2048]{1,0:T(8,128)(2,1)S(1)} %copy-done, bf16[512,2048]{1,0:T(8,128)(2,1)S(1)} %copy-done.15, bf16[2048,256]{1,0:T(8,128)(2,1)} %param.30, f32[512,256]{1,0:T(8,128)} %fusion.132), kind=kOutput, calls=%fused_computation.22 | convolution fusion | flops 1075576832 | bytes 6815744 | tf_op jit(solution)/shard_map/dot_general | solution.py:235
  128.4 5.9 %all-to-all-start.2 = ((bf16[4,128,2048]{2,1,0:T(8,128)(2,1)}), bf16[4,128,2048]{2,1,0:T(8,128)(2,1)S(1)}, u32[]{:S(2)}, u32[]{:S(2)}) async-start(bf16[4,128,2048]{2,1,0:T(8,128)(2,1)} %bitcast.160), calls=%async_computation.2 | async-start | bytes 4194304 | tf_op jit(solution)/shard_map/all_to_all | solution.py:237
  134.3 3.4 %fusion.31 = f32[512,256]{1,0:T(8,128)} fusion(bf16[2048,256]{1,0:T(8,128)(2,1)} %collective-permute-done.1, bf16[64,8,2048]{2,1,0:T(8,128)(2,1)} %all-to-all-done), kind=kOutput, calls=%fused_computation.45 | convolution fusion | flops 536870912 | bytes 3670016 | tf_op jit(solution)/shard_map/dot_general | solution.py:182
  137.7 3.5 %fusion.27 = f32[512,256]{1,0:T(8,128)} fusion(bf16[2048,256]{1,0:T(8,128)(2,1)} %collective-permute-done.4, bf16[64,8,2048]{2,1,0:T(8,128)(2,1)} %all-to-all-done), kind=kOutput, calls=%fused_computation.41 | convolution fusion | flops 536870912 | bytes 3670016 | tf_op jit(solution)/shard_map/dot_general | solution.py:182
  141.2 5.8 %convolution_convert_fusion.3 = bf16[512,2048]{1,0:T(8,128)(2,1)} fusion(bf16[256,2048]{1,0:T(8,128)(2,1)} %collective-permute-done.2, f32[512,256]{1,0:T(8,128)} %fusion.31, bf16[2048,256]{1,0:T(8,128)(2,1)S(1)} %copy-done.7, bf16[64,8,2048]{2,1,0:T(8,128)(2,1)} %all-to-all-done), kind=kOutput, calls=%fused_computation.25 | convolution fusion | flops 1075576832 | bytes 6815744 | tf_op jit(solution)/shard_map/dot_general | solution.py:227
  147.0 6.1 %convolution_convert_fusion.2 = bf16[512,2048]{1,0:T(8,128)(2,1)} fusion(bf16[256,2048]{1,0:T(8,128)(2,1)} %collective-permute-done.5, f32[512,256]{1,0:T(8,128)} %fusion.27, bf16[2048,256]{1,0:T(8,128)(2,1)} %copy-done.8, bf16[64,8,2048]{2,1,0:T(8,128)(2,1)} %all-to-all-done), kind=kOutput, calls=%fused_computation.24 | convolution fusion | flops 1075576832 | bytes 6815744 | tf_op jit(solution)/shard_map/dot_general | solution.py:227
  153.0 3.4 %fusion.37 = f32[512,256]{1,0:T(8,128)} fusion(bf16[64,8,2048]{2,1,0:T(8,128)(2,1)} %all-to-all-done, bf16[1,2048,256]{2,1,0:T(8,128)(2,1)} %param.26), kind=kOutput, calls=%fused_computation.51 | convolution fusion | flops 536870912 | bytes 3670016 | tf_op jit(solution)/shard_map/dot_general | solution.py:181
  156.5 3.4 %fusion.23 = f32[512,256]{1,0:T(8,128)} fusion(bf16[64,8,2048]{2,1,0:T(8,128)(2,1)} %all-to-all-done, bf16[1024,256]{1,0:T(8,128)(2,1)} %collective-permute-done.9, bf16[1024,256]{1,0:T(8,128)(2,1)} %collective-permute-done.8), kind=kOutput, calls=%fused_computation.37 | convolution fusion | flops 538968064 | bytes 3670016 | tf_op jit(solution)/shard_map/dot_general | solution.py:182
  159.9 5.9 %convolution_convert_fusion.4 = bf16[512,2048]{1,0:T(8,128)(2,1)} fusion(bf16[64,8,2048]{2,1,0:T(8,128)(2,1)} %all-to-all-done, f32[512,256]{1,0:T(8,128)} %fusion.37, bf16[1,256,2048]{2,1,0:T(8,128)(2,1)} %param.28, bf16[1,2048,256]{2,1,0:T(8,128)(2,1)} %param.27), kind=kOutput, calls=%fused_computation.26 | convolution fusion | flops 1075576832 | bytes 6815744 | tf_op jit(solution)/shard_map/dot_general | solution.py:227
  165.8 5.3 %collective-permute-done.11 = bf16[128,2048]{1,0:T(8,128)(2,1)S(1)} collective-permute-done((bf16[128,2048]{1,0:T(8,128)(2,1)S(1)}, bf16[128,2048]{1,0:T(8,128)(2,1)S(1)}, u32[]{:S(2)}, u32[]{:S(2)}) %collective-permute-start.11) | collective-permute-done | bytes 524320 | tf_op jit(solution)/shard_map/ppermute | solution.py:174
  171.2 7.7 %fusion.17 = bf16[64,8,2048]{2,1,0:T(8,128)(2,1)} fusion(bf16[512,2048]{1,0:T(8,128)(2,1)} %convolution_convert_fusion.2, bf16[512,2048]{1,0:T(8,128)(2,1)} %convolution_convert_fusion.3, bf16[512,2048]{1,0:T(8,128)(2,1)} %convolution_convert_fusion.4, bf16[128,2048]{1,0:T(8,128)(2,1)S(1)} %collective-permute-done.11, ...), kind=kOutput, calls=%fused_computation.29 | convolution fusion | flops 1088159744 | bytes 13107200 | tf_op jit(solution)/shard_map/dot_general | solution.py:227
  180.3 10.4 %all-to-all-start.1 = ((bf16[64,8,2048]{2,1,0:T(8,128)(2,1)}), bf16[64,8,2048]{2,1,0:T(8,128)(2,1)S(1)}, u32[]{:S(2)}, u32[]{:S(2)}) async-start(bf16[64,8,2048]{2,1,0:T(8,128)(2,1)} %fusion.17), calls=%async_computation.1 | async-start | bytes 4194304 | tf_op jit(solution)/shard_map/all_to_all | solution.py:231
  192.6 3.1 convert_reduce_fusion
  195.7 46.3 %all-to-all-done.1 = bf16[64,8,2048]{2,1,0:T(8,128)(2,1)S(1)} async-done(((bf16[64,8,2048]{2,1,0:T(8,128)(2,1)}), bf16[64,8,2048]{2,1,0:T(8,128)(2,1)S(1)}, u32[]{:S(2)}, u32[]{:S(2)}) %all-to-all-start.1) | async-done | bytes 2097184 | tf_op jit(solution)/shard_map/all_to_all | solution.py:231
  244.5 11.3 %copy.50 = bf16[32,2,256,128]{2,1,0,3:T(2,128)(2,1)} copy(bf16[32,2,256,128]{3,2,0,1:T(8,128)(2,1)} %bitcast.157) | data formatting | bytes 8388608 | tf_op jit(solution)/shard_map/transpose | solution.py:29
  255.9 7.9 %reshape_reshape_reshape.3 = bf16[8,2048,1,2,64]{1,0,4,3,2:T(8,128)(2,1)} reshape(bf16[32,2,256,128]{2,1,0,3:T(2,128)(2,1)} %copy.50) | data formatting | bytes 8388608 | tf_op jit(solution)/shard_map/reshape;reshape;reshape | solution.py:141
  263.8 6.4 %copy.53 = bf16[8,2048,1,2,64]{1,4,3,2,0:T(8,128)(2,1)} copy(bf16[8,2048,1,2,64]{1,0,4,3,2:T(8,128)(2,1)} %reshape_reshape_reshape.3) | data formatting | bytes 8388608
  270.2 55.8 %while.15 = (s32[]{:T(128)}, f32[1,1024]{1,0:T(1,128)S(1)}, f32[1,1024]{1,0:T(1,128)S(1)}, f32[1,1024,64]{1,2,0:T(8,128)}, bf16[8,2048,1,2,64]{1,4,3,2,0:T(8,128...) while((s32[]{:T(128)}, f32[1,1024]{1,0:T(1,128)S(1)}, ...), condition=%wide.region_5.6_spmd.clone, body=%wide.region_2.5_spmd.clone.sunk | while | flops 553849856 | bytes 27590764 | solution.py:142
  274.1 2.3 fusion.154
  280.2 3.2 fusion.154
  287.3 3.2 fusion.154
  294.4 3.2 fusion.154
  301.5 3.2 fusion.154
  308.6 3.2 fusion.154
  315.7 3.2 fusion.154
  322.8 3.2 fusion.154
  (161 shorter events, 64.9 us)
Async XLA Ops:
  7.2 116.3 %copy-start = (bf16[256,2048]{1,0:T(8,128)(2,1)S(1)}, bf16[256,2048]{1,0:T(8,128)(2,1)}, u32[]{:S(2)}) copy-start(bf16[256,2048]{1,0:T(8,128)(2,1)} %param.31) | copy-start | bytes 3145732
  10.6 2.1 copy-start.3
  12.7 18.9 %copy-start.9 = (bf16[256,64]{0,1:T(8,128)(2,1)S(1)}, bf16[256,64]{0,1:T(8,128)(2,1)}, u32[]{:S(2)}) copy-start(bf16[256,64]{0,1:T(8,128)(2,1)} %param.18) | copy-start | bytes 98308
  12.7 48.8 %copy-start.13 = (f32[64]{0:T(128)S(1)}, f32[64]{0:T(128)}, u32[]{:S(2)}) copy-start(f32[64]{0:T(128)} %param.21) | copy-start | bytes 772
  12.7 49.2 %copy-start.11 = (bf16[256,64]{0,1:T(8,128)(2,1)S(1)}, bf16[256,64]{0,1:T(8,128)(2,1)}, u32[]{:S(2)}) copy-start(bf16[256,64]{0,1:T(8,128)(2,1)} %param.19) | copy-start | bytes 98308
  12.7 115.7 %all-to-all-start = ((bf16[64,8,2048]{2,1,0:T(8,128)(2,1)}), bf16[64,8,2048]{2,1,0:T(8,128)(2,1)}, u32[]{:S(2)}, u32[]{:S(2)}) async-start(bf16[64,8,2048]{2,1,0:T(8,128)(2,1)} %fusion.16), calls=%async_computation | async-start | bytes 4194304 | tf_op jit(solution)/shard_map/all_to_all | solution.py:218
  25.1 94.8 %all-gather.7.cloned.1.call-start = ((), (), s32[]{:S(2)}) async-start(), calls=%async_computation.4 | async-start | bytes 2621440 | tf_op jit(solution)/shard_map/all_gather | solution.py:233
  25.8 165.2 %all-gather.5.cloned.1.call-start = ((), (), s32[]{:S(2)}) async-start(), calls=%async_computation.3 | async-start | bytes 2162688 | tf_op jit(solution)/shard_map/all_gather | solution.py:26
  25.8 35.0 %collective-permute-start = (bf16[2048,256]{1,0:T(8,128)(2,1)}, bf16[2048,256]{1,0:T(8,128)(2,1)S(1)}, u32[]{:S(2)}, u32[]{:S(2)}) collective-permute-start(bf16[2048,256]{1,0:T(8,128)(2,1)} %bitcast.24), channel_id=1, source_target_pairs={{0,1},{1,2},{2,3},{3,0},{4,5},{5,6},{6,7},{7,4},{8,9},{9,10},{10,1... | collective-permute-start | bytes 3145736 | tf_op jit(solution)/shard_map/ppermute | solution.py:169
  27.5 36.1 %collective-permute-start.3 = (bf16[2048,256]{1,0:T(8,128)(2,1)}, bf16[2048,256]{1,0:T(8,128)(2,1)S(1)}, u32[]{:S(2)}, u32[]{:S(2)}) collective-permute-start(bf16[2048,256]{1,0:T(8,128)(2,1)} %bitcast.24), channel_id=1, source_target_pairs={{0,3},{1,0},{2,1},{3,2},{4,7},{5,4},{6,5},{7,6},{8,11},{9,8},{10,9... | collective-permute-start | bytes 3145736 | tf_op jit(solution)/shard_map/ppermute | solution.py:170
  27.9 63.6 %collective-permute-start.1 = (bf16[2048,256]{1,0:T(8,128)(2,1)}, bf16[2048,256]{1,0:T(8,128)(2,1)}, u32[]{:S(2)}, u32[]{:S(2)}) collective-permute-start(bf16[2048,256]{1,0:T(8,128)(2,1)} %bitcast.172), channel_id=1, source_target_pairs={{0,1},{1,2},{2,3},{3,0},{4,5},{5,6},{6,7},{7,4},{8,9},{9,10},{10,1... | collective-permute-start | bytes 3145736 | tf_op jit(solution)/shard_map/ppermute | solution.py:169
  29.5 65.6 %collective-permute-start.4 = (bf16[2048,256]{1,0:T(8,128)(2,1)}, bf16[2048,256]{1,0:T(8,128)(2,1)}, u32[]{:S(2)}, u32[]{:S(2)}) collective-permute-start(bf16[2048,256]{1,0:T(8,128)(2,1)} %bitcast.173), channel_id=1, source_target_pairs={{0,3},{1,0},{2,1},{3,2},{4,7},{5,4},{6,5},{7,6},{8,11},{9,8},{10,9... | collective-permute-start | bytes 3145736 | tf_op jit(solution)/shard_map/ppermute | solution.py:170
  30.0 84.1 %collective-permute-start.2 = (bf16[256,2048]{1,0:T(8,128)(2,1)}, bf16[256,2048]{1,0:T(8,128)(2,1)}, u32[]{:S(2)}, u32[]{:S(2)}) collective-permute-start(bf16[256,2048]{1,0:T(8,128)(2,1)} %bitcast.170), channel_id=1, source_target_pairs={{0,1},{1,2},{2,3},{3,0},{4,5},{5,6},{6,7},{7,4},{8,9},{9,10},{10,1... | collective-permute-start | bytes 3145736 | tf_op jit(solution)/shard_map/ppermute | solution.py:169
  60.9 36.5 %copy-start.6 = (bf16[2048,256]{1,0:T(8,128)(2,1)}, bf16[2048,256]{1,0:T(8,128)(2,1)S(1)}, u32[]{:S(2)}) copy-start(bf16[2048,256]{1,0:T(8,128)(2,1)S(1)} %collective-permute-done) | copy-start | bytes 3145732
  60.9 56.8 %collective-permute-start.5 = (bf16[256,2048]{1,0:T(8,128)(2,1)}, bf16[256,2048]{1,0:T(8,128)(2,1)}, u32[]{:S(2)}, u32[]{:S(2)}) collective-permute-start(bf16[256,2048]{1,0:T(8,128)(2,1)} %bitcast.171), channel_id=1, source_target_pairs={{0,3},{1,0},{2,1},{3,2},{4,7},{5,4},{6,5},{7,6},{8,11},{9,8},{10,9... | collective-permute-start | bytes 3145736 | tf_op jit(solution)/shard_map/ppermute | solution.py:170
  63.6 54.0 %copy-start.8 = (bf16[2048,256]{1,0:T(8,128)(2,1)}, bf16[2048,256]{1,0:T(8,128)(2,1)S(1)}, u32[]{:S(2)}) copy-start(bf16[2048,256]{1,0:T(8,128)(2,1)S(1)} %collective-permute-done.3) | copy-start | bytes 3145732
  63.6 102.2 %collective-permute-start.6 = (bf16[1024,256]{1,0:T(8,128)(2,1)}, bf16[1024,256]{1,0:T(8,128)(2,1)}, u32[]{:S(2)}, u32[]{:S(2)}) collective-permute-start(bf16[1024,256]{1,0:T(8,128)(2,1)} %slice.70), channel_id=1, source_target_pairs={{0,1},{1,2},{2,3},{3,0},{4,5},{5,6},{6,7},{7,4},{8,9},{9,10},{10,1... | collective-permute-start | bytes 1572872 | tf_op jit(solution)/shard_map/ppermute | solution.py:173
  91.6 74.2 %collective-permute-start.7 = (bf16[1024,256]{1,0:T(8,128)(2,1)}, bf16[1024,256]{1,0:T(8,128)(2,1)}, u32[]{:S(2)}, u32[]{:S(2)}) collective-permute-start(bf16[1024,256]{1,0:T(8,128)(2,1)} %slice.71), channel_id=1, source_target_pairs={{0,3},{1,0},{2,1},{3,2},{4,7},{5,4},{6,5},{7,6},{8,11},{9,8},{10,9... | collective-permute-start | bytes 1572872 | tf_op jit(solution)/shard_map/ppermute | solution.py:174
  95.1 61.3 %collective-permute-start.8 = (bf16[1024,256]{1,0:T(8,128)(2,1)}, bf16[1024,256]{1,0:T(8,128)(2,1)}, u32[]{:S(2)}, u32[]{:S(2)}) collective-permute-start(bf16[1024,256]{1,0:T(8,128)(2,1)} %slice.72), channel_id=1, source_target_pairs={{0,1},{1,2},{2,3},{3,0},{4,5},{5,6},{6,7},{7,4},{8,9},{9,10},{10,1... | collective-permute-start | bytes 1572872 | tf_op jit(solution)/shard_map/ppermute | solution.py:173
  114.1 42.5 %collective-permute-start.9 = (bf16[1024,256]{1,0:T(8,128)(2,1)}, bf16[1024,256]{1,0:T(8,128)(2,1)}, u32[]{:S(2)}, u32[]{:S(2)}) collective-permute-start(bf16[1024,256]{1,0:T(8,128)(2,1)} %slice.73), channel_id=1, source_target_pairs={{0,3},{1,0},{2,1},{3,2},{4,7},{5,4},{6,5},{7,6},{8,11},{9,8},{10,9... | collective-permute-start | bytes 1572872 | tf_op jit(solution)/shard_map/ppermute | solution.py:174
  117.6 48.2 %collective-permute-start.10 = (bf16[128,2048]{1,0:T(8,128)(2,1)}, bf16[128,2048]{1,0:T(8,128)(2,1)}, u32[]{:S(2)}, u32[]{:S(2)}) collective-permute-start(bf16[128,2048]{1,0:T(8,128)(2,1)} %slice.74), channel_id=1, source_target_pairs={{0,1},{1,2},{2,3},{3,0},{4,5},{5,6},{6,7},{7,4},{8,9},{9,10},{10,1... | collective-permute-start | bytes 1572872 | tf_op jit(solution)/shard_map/ppermute | solution.py:173
  119.9 3.5 %copy-start.15 = (bf16[512,2048]{1,0:T(8,128)(2,1)S(1)}, bf16[512,2048]{1,0:T(8,128)(2,1)}, u32[]{:S(2)}) copy-start(bf16[512,2048]{1,0:T(8,128)(2,1)} %all-gather.7.cloned.1.call-done) | copy-start | bytes 6291460
  128.4 50.5 %all-to-all-start.2 = ((bf16[4,128,2048]{2,1,0:T(8,128)(2,1)}), bf16[4,128,2048]{2,1,0:T(8,128)(2,1)S(1)}, u32[]{:S(2)}, u32[]{:S(2)}) async-start(bf16[4,128,2048]{2,1,0:T(8,128)(2,1)} %bitcast.160), calls=%async_computation.2 | async-start | bytes 4194304 | tf_op jit(solution)/shard_map/all_to_all | solution.py:237
  137.7 3.5 %copy-start.7 = (bf16[2048,256]{1,0:T(8,128)(2,1)S(1)}, bf16[2048,256]{1,0:T(8,128)(2,1)}, u32[]{:S(2)}) copy-start(bf16[2048,256]{1,0:T(8,128)(2,1)} %copy-done.6) | copy-start | bytes 3145732
  153.0 3.4 %copy-start.5 = (bf16[128,2048]{1,0:T(8,128)(2,1)S(1)}, bf16[128,2048]{1,0:T(8,128)(2,1)}, u32[]{:S(2)}) copy-start(bf16[128,2048]{1,0:T(8,128)(2,1)} %slice.75) | copy-start | bytes 1572868
  156.5 14.7 %collective-permute-start.11 = (bf16[128,2048]{1,0:T(8,128)(2,1)S(1)}, bf16[128,2048]{1,0:T(8,128)(2,1)S(1)}, u32[]{:S(2)}, u32[]{:S(2)}) collective-permute-start(bf16[128,2048]{1,0:T(8,128)(2,1)S(1)} %copy-done.5), channel_id=1, source_target_pairs={{0,3},{1,0},{2,1},{3,2},{4,7},{5,4},{6,5},{7,6},{8,11},{9,8},{10,9... | collective-permute-start | bytes 1572872 | tf_op jit(solution)/shard_map/ppermute | solution.py:174
  178.9 1.4 copy-start.2
  180.3 61.7 %all-to-all-start.1 = ((bf16[64,8,2048]{2,1,0:T(8,128)(2,1)}), bf16[64,8,2048]{2,1,0:T(8,128)(2,1)S(1)}, u32[]{:S(2)}, u32[]{:S(2)}) async-start(bf16[64,8,2048]{2,1,0:T(8,128)(2,1)} %fusion.17), calls=%async_computation.1 | async-start | bytes 4194304 | tf_op jit(solution)/shard_map/all_to_all | solution.py:231
  190.7 1.3 copy-start.12
  190.7 53.8 %all-gather.9.cloned.1.call-start = ((), (), s32[]{:S(2)}) async-start(), calls=%async_computation.5 | async-start | bytes 6291456 | tf_op jit(solution)/shard_map/all_gather | solution.py:26
  242.0 1.2 copy-start.4
  326.0 1.9 copy-start.1
  (2 other events, 2.0 us)
Sparse Core Ops, SparseCore 0:
  28.3 50.4 all-gather.6
  81.9 78.9 all-gather.4
  193.3 19.3 all-gather.8

commit v2 on v1

v2 whole, which is shorter than its diff:
```python
import functools

import jax
import jax.numpy as jnp
from jax import lax
from jax.experimental import pallas as pl
from jax.experimental.pallas import tpu as pltpu
from jax.sharding import Mesh
from jax.sharding import PartitionSpec as P

GRID_W = 64
EP = ("ep_0", "ep_1", "ep_2")
EP_TP = ("ep_0", "ep_1", "ep_2", "tp")
MESH_ID = pl.DeviceIdType.MESH
Z, X, CORE, Y = EP_TP


epsilon = 1e-06
rotary_base = 10000.0
routed_scale = 2.5


def lane_places(heads, size, offset):
    source = jnp.arange(heads * size)[None, :, None]
    lane = jnp.arange(128)[None, None, :] - offset
    head = jnp.arange(heads)[:, None, None]
    inside = (lane >= 0) & (lane < size)
    straight = inside & (source == head * size + lane)
    swapped = inside & (source == head * size + (lane ^ 1))
    return straight.astype(jnp.bfloat16), swapped.astype(jnp.bfloat16)


def rotated(rows_in, gain, heads, size, positions):
    straight, swapped = lane_places(heads, size, 0)
    own = jnp.einsum("td,hde->hte", rows_in, straight, preferred_element_type=jnp.float32)
    other = jnp.einsum("td,hde->hte", rows_in, swapped, preferred_element_type=jnp.float32)
    lane = jnp.arange(128)
    wide = jnp.pad(gain, (0, 128 - size))
    wide_swapped = jnp.pad(gain.reshape(-1, 2)[:, ::-1].reshape(-1), (0, 128 - size))
    factor = lax.rsqrt(jnp.sum(own * own, axis=-1, keepdims=True) / size + epsilon)
    pair_count = size // 4
    pair = (lane // 2) % (2 * pair_count)
    inv_freq = rotary_base ** (-(pair % pair_count).astype(jnp.float32) / pair_count)
    grid_row = (positions // GRID_W).astype(jnp.float32)[:, None]
    grid_col = (positions % GRID_W).astype(jnp.float32)[:, None]
    angles = jnp.where(pair[None, :] < pair_count, grid_row, grid_col) * inv_freq[None, :]
    sign = jnp.where(lane % 2 == 0, -1.0, 1.0)
    turned = (own * factor * wide) * jnp.cos(angles) + (other * factor * wide_swapped) * (
        sign * jnp.sin(angles)
    )
    return turned.astype(jnp.bfloat16)


def attention_kernel(
    q_ref, kv_ref, gate_ref, up_ref,
    out_ref, gates_ref, ups_ref,
    buf, run_max, run_sum, mixed,
    z_send, z_recv, x_send, x_recv, c_send, c_recv, w_send, w_recv, own_sem,
):
    z, x, core, y = (lax.axis_index(name) for name in EP_TP)
    z_size, x_size, y_size = buf.shape[2], buf.shape[1], 4
    half = gate_ref.shape[0] // 2
    block_half = z_size // 2

    def near(index, step, size):
        return lax.rem(index + step + size, size)

    x_right, x_left, x_far = near(x, 1, x_size), near(x, -1, x_size), near(x, 2, x_size)
    y_right, y_left = near(y, 1, y_size), near(y, -1, y_size)
    barrier = pltpu.get_barrier_semaphore()
    peers = [{Z: near(z, k, z_size)} for k in range(1, z_size)]
    peers += [{X: x_right}, {X: x_left}, {CORE: 1 - core}, {Y: y_right}, {Y: y_left}]
    for peer in peers:
        pl.semaphore_signal(barrier, inc=1, device_id=peer, device_id_type=MESH_ID)
    pl.semaphore_wait(barrier, len(peers))

    def remote(src, dst, send_sem, recv_sem, peer):
        return pltpu.make_async_remote_copy(
            src_ref=src, dst_ref=dst, send_sem=send_sem, recv_sem=recv_sem,
            device_id=peer, device_id_type=MESH_ID,
        )

    weights = []
    for n, (source, slots) in enumerate(((gate_ref, gates_ref), (up_ref, ups_ref))):
        to_right = remote(source, slots.at[0], w_send.at[n, 0], w_recv.at[n, 0], {Y: y_right})
        to_left = remote(source, slots.at[1], w_send.at[n, 1], w_recv.at[n, 1], {Y: y_left})
        first, second = pl.ds(0, half), pl.ds(half, half)
        on_right = remote(
            slots.at[0, first], slots.at[2, first], w_send.at[n, 2], w_recv.at[n, 2], {Y: y_right}
        )
        on_left = remote(
            slots.at[1, second], slots.at[2, second], w_send.at[n, 3], w_recv.at[n, 3], {Y: y_left}
        )
        weights.append((to_right, to_left, on_right, on_left))
    for to_right, to_left, _, _ in weights:
        to_right.start()
        to_left.start()

    along_z = [
        remote(kv_ref, buf.at[core, x, z], z_send.at[k], z_recv.at[k], {Z: near(z, k, z_size)})
        for k in range(1, z_size)
    ]
    for copy in along_z:
        copy.start()
    own = pltpu.make_async_copy(kv_ref, buf.at[core, x, z], own_sem)
    own.start()
    run_max[...] = jnp.full_like(run_max, -jnp.inf)
    run_sum[...] = jnp.zeros_like(run_sum)
    mixed[...] = jnp.zeros_like(mixed)
    own.wait()
    for copy in along_z:
        copy.wait_recv()

    def attend(which_core, which_x):
        keys = buf.shape[2] * buf.shape[3]

        def tile(i, carry):
            rows = pl.ds(i * TILE, TILE)
            span = buf[which_core, which_x].reshape(keys, 128)
            scores = lax.dot_general(
                q_ref[rows, :], span, (((1,), (1,)), ((), ())), preferred_element_type=jnp.float32
            )
            old_max = run_max[rows, :]
            new_max = jnp.maximum(old_max, jnp.max(scores, axis=1, keepdims=True))
            factor = jnp.exp(old_max - new_max)
            weights_now = jnp.exp(scores - new_max[:, :1])
            run_sum[rows, :] = run_sum[rows, :] * factor + jnp.sum(
                weights_now, axis=1, keepdims=True
            )
            mixed[rows, :] = mixed[rows, :] * factor + jnp.dot(
                weights_now.astype(jnp.bfloat16), span, preferred_element_type=jnp.float32
            )
            run_max[rows, :] = new_max
            return carry

        lax.fori_loop(0, q_ref.shape[0] // TILE, tile, 0)

    def line_to_core(which_x, slot):
        return remote(
            buf.at[core, which_x], buf.at[core, which_x], c_send.at[slot], c_recv.at[slot],
            {CORE: 1 - core},
        )

    line = buf.at[core, x]
    to_right = remote(line, line, x_send.at[0], x_recv.at[0], {X: x_right})
    to_left = remote(line, line, x_send.at[1], x_recv.at[1], {X: x_left})
    first, second = pl.ds(0, block_half), pl.ds(block_half, block_half)
    on_right = remote(
        buf.at[core, x_left, first], buf.at[core, x_left, first],
        x_send.at[2], x_recv.at[2], {X: x_right},
    )
    on_left = remote(
        buf.at[core, x_right, second], buf.at[core, x_right, second],
        x_send.at[3], x_recv.at[3], {X: x_left},
    )
    lines = [line_to_core(which, n) for n, which in enumerate((x, x_left, x_right, x_far))]
    to_right.start()
    to_left.start()
    lines[0].start()
    attend(core, x)
    lines[0].wait_recv()
    attend(1 - core, x)
    to_right.wait_recv()
    on_right.start()
    lines[1].start()
    to_left.wait_recv()
    on_left.start()
    lines[2].start()
    attend(core, x_left)
    weights[0][0].wait_recv()
    weights[0][2].start()
    weights[0][1].wait_recv()
    weights[0][3].start()
    attend(core, x_right)
    on_right.wait_recv()
    on_left.wait_recv()
    lines[3].start()
    lines[1].wait_recv()
    attend(1 - core, x_left)
    weights[1][0].wait_recv()
    weights[1][2].start()
    weights[1][1].wait_recv()
    weights[1][3].start()
    lines[2].wait_recv()
    attend(1 - core, x_right)
    attend(core, x_far)
    lines[3].wait_recv()
    attend(1 - core, x_far)
    out_ref[...] = (mixed[...] / run_sum[...]).astype(out_ref.dtype)
    for group in weights:
        group[2].wait_recv()
        group[3].wait_recv()
        for copy in group:
            copy.wait_send()
    for copy in along_z + [to_right, to_left, on_right, on_left] + lines:
        copy.wait_send()


TILE = 256


def attend_and_gather(q_rows, key_value, w_gate, w_up):
    rows = q_rows.shape[0]
    tokens = key_value.shape[0]
    z_size, x_size, cores = (lax.axis_size(name) for name in EP)
    dma = pltpu.SemaphoreType.DMA
    slots = jax.ShapeDtypeStruct((3, *w_gate.shape), w_gate.dtype)
    vmem, anywhere = pl.BlockSpec(memory_space=pltpu.VMEM), pl.BlockSpec(memory_space=pl.ANY)
    keys = tokens * z_size * x_size * cores
    return pl.pallas_call(
        attention_kernel,
        out_shape=[jax.ShapeDtypeStruct((rows, 128), jnp.bfloat16), slots, slots],
        in_specs=[vmem, vmem, anywhere, anywhere],
        out_specs=[vmem, anywhere, anywhere],
        scratch_shapes=[
            pltpu.VMEM((cores, x_size, z_size, tokens, 128), jnp.bfloat16),
            pltpu.VMEM((rows, 128), jnp.float32),
            pltpu.VMEM((rows, 128), jnp.float32),
            pltpu.VMEM((rows, 128), jnp.float32),
            dma((z_size,)), dma((z_size,)),
            dma((4,)), dma((4,)),
            dma((4,)), dma((4,)),
            dma((2, 4)), dma((2, 4)),
            dma,
        ],
        compiler_params=pltpu.CompilerParams(
            collective_id=0, has_side_effects=True, vmem_limit_bytes=40 * 1024 * 1024
        ),
        cost_estimate=pl.CostEstimate(
            flops=60 * rows * keys * 128 // 2, bytes_accessed=2 * keys * 256, transcendentals=0
        ),
        name="attend_and_gather",
    )(q_rows, key_value, w_gate, w_up)


def ring(step):
    return [(i, (i + step) % 4) for i in range(4)]


def token_slots(own_routes, capacity):
    rows = own_routes.shape[0]
    earlier = jnp.arange(rows)[:, None] < jnp.arange(rows)[None, :]
    slots = []
    for k in range(own_routes.shape[1]):
        mine = own_routes[:, k]
        same = own_routes[:, 0][:, None] == mine[None, :]
        for other in range(1, own_routes.shape[1]):
            same = same | (own_routes[:, other][:, None] == mine[None, :])
        rank = jnp.sum((same & earlier).astype(jnp.int32), axis=0)
        slots.append(mine * capacity + rank)
    return slots


def from_ring(array):
    half = array.shape[0] // 2
    left = lax.ppermute(array, "tp", ring(1))
    right = lax.ppermute(array, "tp", ring(3))
    far = jnp.concatenate(
        [
            lax.ppermute(left[:half], "tp", ring(1)),
            lax.ppermute(right[half:], "tp", ring(3)),
        ]
    )
    return [array, left, right, far]


def hidden_rows(rows_in, w_gate, w_up):
    gate_proj = jnp.dot(rows_in, w_gate, preferred_element_type=jnp.float32)
    up_proj = jnp.dot(rows_in, w_up, preferred_element_type=jnp.float32)
    return (jax.nn.silu(gate_proj) * up_proj).astype(jnp.bfloat16)


def dispatch(
    moe_tokens,
    norm_gain,
    routes,
    route_weights,
):
    tok_rows, model_width = moe_tokens.shape
    top_count = routes.shape[1]
    ep_size = lax.axis_size(EP)
    experts = ep_size
    capacity = 2 * tok_rows * top_count // experts
    lane = lax.axis_index("tp")
    values32 = moe_tokens.astype(jnp.float32)
    normed = (
        values32
        * lax.rsqrt(jnp.mean(values32 * values32, axis=-1, keepdims=True) + epsilon)
        * norm_gain
    ).astype(jnp.bfloat16)
    own_routes = lax.dynamic_slice_in_dim(routes, lane * tok_rows, tok_rows, 0)
    own_weights = lax.dynamic_slice_in_dim(route_weights, lane * tok_rows, tok_rows, 0)
    gates = own_weights / jnp.sum(own_weights, axis=-1, keepdims=True) * routed_scale
    slots = token_slots(own_routes, capacity)
    places = jnp.arange(experts * capacity, dtype=jnp.int32)
    one_hots = [(places[:, None] == slot[None, :]).astype(jnp.bfloat16) for slot in slots]
    placed = one_hots[0] + one_hots[1]
    send = jnp.dot(placed, normed, preferred_element_type=jnp.float32).astype(jnp.bfloat16)
    arrived = lax.all_to_all(
        send.reshape(experts, capacity, model_width), EP, split_axis=0, concat_axis=0, tiled=True
    ).reshape(experts * capacity, model_width)
    return normed, arrived, one_hots, gates


def experts_half(
    dispatched,
    gates_got,
    ups_got,
    expert_gate,
    expert_up,
    expert_down,
    shared_gate,
    shared_up,
    shared_down,
):
    normed, arrived, one_hots, gates = dispatched
    tok_rows, model_width = normed.shape
    experts = lax.axis_size(EP)
    capacity = arrived.shape[0] // experts
    top_count = len(one_hots)
    gate_parts = [expert_gate[0], gates_got[0], gates_got[1], gates_got[2]]
    up_parts = [expert_up[0], ups_got[0], ups_got[1], ups_got[2]]
    down_parts = from_ring(expert_down[0])
    total = None
    for w_gate, w_up, w_down in zip(gate_parts, up_parts, down_parts):
        hidden = hidden_rows(arrived, w_gate, w_up)
        part = jnp.dot(hidden, w_down, preferred_element_type=jnp.float32)
        part = part.astype(jnp.bfloat16).astype(jnp.float32)
        total = part if total is None else total + part
    outgoing = total.astype(jnp.bfloat16).reshape(experts, capacity, model_width)
    returned = lax.all_to_all(outgoing, EP, split_axis=0, concat_axis=0, tiled=True)
    returned = returned.reshape(experts * capacity, model_width)
    group_rows = lax.all_gather(normed, "tp", axis=0, tiled=True)
    shared_hidden = hidden_rows(group_rows, shared_gate, shared_up)
    shared_part = jnp.dot(shared_hidden, shared_down, preferred_element_type=jnp.float32)
    shared_part = shared_part.astype(jnp.bfloat16).reshape(4, tok_rows, model_width)
    shared_got = lax.all_to_all(shared_part, "tp", split_axis=0, concat_axis=0, tiled=True)
    shared_sum = jnp.sum(shared_got.astype(jnp.float32), axis=0)
    routed_total = 0.0
    for k in range(top_count):
        picked = lax.dot_general(
            one_hots[k], returned, (((0,), (0,)), ((), ())), preferred_element_type=jnp.float32
        )
        routed_total = routed_total + gates[:, k : k + 1] * picked
    return (routed_total + shared_sum).astype(jnp.bfloat16)


def body(
    query_rows,
    key_rows,
    value_rows,
    query_gain,
    key_gain,
    moe_tokens,
    norm_gain,
    routes,
    route_weights,
    expert_gate,
    expert_up,
    expert_down,
    shared_gate,
    shared_up,
    shared_down,
):
    dispatched = dispatch(moe_tokens, norm_gain, routes, route_weights)
    row_count = query_rows.shape[0]
    size = query_gain.shape[0]
    heads = query_rows.shape[1] // size
    positions = lax.axis_index(EP) * row_count + jnp.arange(row_count, dtype=jnp.int32)
    q_rot = rotated(query_rows, query_gain, heads, size, positions) * jnp.bfloat16(size**-0.5)
    k_rot = rotated(key_rows, key_gain, 1, size, positions)[0]
    placed = lane_places(1, size, size)[0][0]
    values = jnp.dot(value_rows, placed, preferred_element_type=jnp.float32).astype(jnp.bfloat16)
    attn, gates_got, ups_got = attend_and_gather(
        q_rot.reshape(heads * row_count, 128), k_rot + values, expert_gate[0], expert_up[0]
    )
    attn_out = attn[:, size:].reshape(heads, row_count, size).transpose(1, 0, 2)
    attn_out = attn_out.reshape(row_count, heads * size)
    moe_out = experts_half(
        dispatched,
        gates_got,
        ups_got,
        expert_gate,
        expert_up,
        expert_down,
        shared_gate,
        shared_up,
        shared_down,
    )
    return (attn_out, moe_out)


def solution(mesh):
    finer = Mesh(mesh.devices.reshape(8, 4, 2, mesh.shape["tp"]), ("ep_0", "ep_1", "ep_2", "tp"))
    return jax.shard_map(
        body,
        mesh=finer,
        in_specs=(
            P(EP, "tp"),
            P(EP, "tp"),
            P(EP, "tp"),
            P(),
            P(),
            P(EP_TP, None),
            P(),
            P(EP, None),
            P(EP, None),
            P(EP, None, "tp"),
            P(EP, None, "tp"),
            P(EP, "tp", None),
            P(None, "tp"),
            P(None, "tp"),
            P("tp", None),
        ),
        out_specs=(P(EP, "tp"), P(EP_TP, None)),
        check_vma=False,
    )
```

time: 336 us -> 265 us (0.79)
  Pallas kernels: 0 us -> 100 us
  waiting for transfers between devices: 124 us -> 48 us
  local copies, waits for them, and re-layouts: 48.8 us -> 9.21 us
  matrix products: 86.7 us -> 55.7 us
  other arithmetic: 19.3 us -> 6.19 us
  starting transfers between devices: 40.8 us -> 30.1 us
    pallas_call x0 -> x1, Pallas kernels: none -> 100 us  [attend_and_gather(): pl.pallas_call(attention_kernel, out_shape=[jax.ShapeDtypeStruct((rows, 1...]
    ppermute x3 -> x1, waiting for transfers between devices: 71.7 us -> 0.01 us  [from_ring(): left = lax.ppermute(array, 'tp', ring(1))]
    dot_general x20 -> x6, matrix products: 47.5 us -> 4.84 us  [the longest x1 3.09 us: dispatch(): jnp.dot(placed, normed, preferred_element_type=jnp.float32)]
    reduce_sum x12 -> x2, other arithmetic: 12.9 us -> 1.25 us  [the longest x1 1.23 us: dispatch(): jnp.mean(values32 * values32, axis=-1, keepdims=True) + epsilon]
    transpose x2 -> x0, local copies, waits for them, and re-layouts: 11.3 us -> none  [the longest x1 11.3 us: stacked_from(): pieces = pieces.transpose(*back, *range(len(axes), pieces.ndim))]
    another operation x4 -> x0, local copies, waits for them, and re-layouts: 8.77 us -> none  [the longest x1 7.89 us: attend(): piece_rows.reshape(piece_count // length, length, kv_heads, 2, head_size)]
    squeeze x8 -> x0, local copies, waits for them, and re-layouts: 8.64 us -> none  [attend(): carried, unused = lax.scan(one_span, carried, spans)]
    dot_general x2 -> x5, matrix products: 6.95 us -> 15.1 us  [hidden_rows(): gate_proj = jnp.dot(rows_in, w_gate, preferred_element_type=jnp.float32)]
  transfers between devices with their start and end apart: 18 -> 8, of which waited for: 5 -> 1; matrix products, arithmetic and copies ran while one was open for 19% -> 23% of each run, Pallas kernels for 0% -> 38%
where the time goes in v2:
time: 265 us; the launch traced here: 264 us
  Pallas kernels  100 us (38%)
  matrix products  55.7 us (21%)
  waiting for transfers between devices  48 us (18%)
  starting transfers between devices  30.1 us (11%)
  between operations  14.4 us (5%)
  local copies, waits for them, and re-layouts  9.21 us (3%)
  other arithmetic  6.19 us (2%)
    pallas_call x1, Pallas kernels, attend_and_gather(): pl.pallas_call(attention_kernel, out_shape=[jax.ShapeDtypeStruct((rows, 1...  100 us
    all_to_all x1, waiting for transfers between devices, experts_half(): lax.all_to_all(outgoing, EP, split_axis=0, concat_axis=0, tiled=True)  48 us
    dot_general x4, matrix products, experts_half(): part = jnp.dot(hidden, w_down, preferred_element_type=jnp.float32)  25.2 us
    dot_general x5, matrix products, hidden_rows(): gate_proj = jnp.dot(rows_in, w_gate, preferred_element_type=jnp.float32)  15.1 us
    all_to_all x1, starting transfers between devices, dispatch(): lax.all_to_all(send.reshape(experts, capacity, model_width), EP, split_ax...  12.3 us
    all_to_all x1, starting transfers between devices, experts_half(): lax.all_to_all(shared_part, 'tp', split_axis=0, concat_axis=0, tiled=True)  7.31 us
    all_to_all x1, starting transfers between devices, experts_half(): lax.all_to_all(outgoing, EP, split_axis=0, concat_axis=0, tiled=True)  5.7 us
    dot_general x1, matrix products, experts_half(): jnp.dot(shared_hidden, shared_down, preferred_element_type=jnp.float32)  5.65 us
  transfers between devices with their start and end apart: 8, of which 1 were waited for; matrix products, arithmetic and copies ran while one was open for 23% of the time, Pallas kernels for 38%

profile of v2, /device:TPU:8, one launch (start us, length us, event | category | flops | bytes accessed | tf_op | source)
XLA Modules:
  0.0 264.0 jit_solution(12581625452127761688)
XLA Ops:
  7.2 1.7 collective-permute-start
  8.9 0.7 collective-permute-start.1
  9.6 1.2 fusion.69
  10.8 2.0 fusion.71
  12.8 0.7 constant_dynamic-slice_fusion
  13.7 3.1 %fusion = bf16[64,8,2048]{2,1,0:T(8,128)(2,1)} fusion(bf16[128,2048]{1,0:T(8,128)(2,1)} %fusion.71, s32[128]{0:T(128)S(1)} %get-tuple-element.19, s32[128]{0:T(128)S(1)} %get-tuple-element.18), kind=kOutput, calls=%fused_computation.8 | convolution fusion | flops 270008320 | bytes 2622464 | tf_op jit(solution)/shard_map/dot_general | solution.py:298
  16.8 12.3 %all-to-all-start = ((bf16[64,8,2048]{2,1,0:T(8,128)(2,1)}), bf16[64,8,2048]{2,1,0:T(8,128)(2,1)}, u32[]{:S(2)}, u32[]{:S(2)}) async-start(bf16[64,8,2048]{2,1,0:T(8,128)(2,1)} %fusion), calls=%async_computation | async-start | bytes 4194304 | tf_op jit(solution)/shard_map/all_to_all | solution.py:299
  31.6 0.6 fusion.68
  32.5 1.2 copy-done.2
  33.7 100.4 %attend_and_gather.1 = (bf16[1024,128]{1,0:T(8,128)(2,1)S(1)}, bf16[3,2048,256]{2,1,0:T(8,128)(2,1)S(1)}, bf16[3,2048,256]{2,1,0:T(8,128)(2,1)S(1)}) custom-call(bf16[1024,128]{1,0:T(8,128)(2,1)S(1)} %bitcast.170, bf16[256,128]{1,0:T(8,128)(2,1)S(1)} %fusion.67.kv_ref, bf16[2048,256]{1,0:T(8,128)(2,1)S(1)} %bitcast.171, bf16[2048,256]{1,0:T(8,128)(2,1)S(1)} %bitcast.172), custom_call_target="tpu_custom_call" | custom-call | flops 64424509440 | bytes 8388608 | tf_op jit(solution)/shard_map/attend_and_gather/pallas_call | solution.py:210
  134.2 1.7 copy-done.4
  135.8 1.7 copy-done.5
  137.5 1.1 slice.56
  138.6 1.9 collective-permute-start.2
  140.4 1.1 slice.57
  142.1 3.4 %fusion.178 = f32[512,256]{1,0:T(8,128)} fusion(bf16[512,2048]{1,0:T(8,128)(2,1)} %all-gather.2.cloned.1.call-done, bf16[2048,256]{1,0:T(8,128)(2,1)} %param.27), kind=kOutput, calls=%fused_computation.212 | convolution fusion | flops 536870912 | bytes 3670016 | tf_op jit(solution)/shard_map/dot_general | solution.py:268
  145.4 5.7 %convolution_convert_fusion = bf16[512,2048]{1,0:T(8,128)(2,1)} fusion(bf16[256,2048]{1,0:T(8,128)(2,1)S(1)} %copy-done, bf16[512,2048]{1,0:T(8,128)(2,1)} %all-gather.2.cloned.1.call-done, bf16[2048,256]{1,0:T(8,128)(2,1)} %param.28, f32[512,256]{1,0:T(8,128)} %fusion.178), kind=kOutput, calls=%fused_computation.2 | convolution fusion | flops 1075576832 | bytes 6815744 | tf_op jit(solution)/shard_map/dot_general | solution.py:335
  151.1 7.3 %all-to-all-start.2 = ((bf16[4,128,2048]{2,1,0:T(8,128)(2,1)}), bf16[4,128,2048]{2,1,0:T(8,128)(2,1)}, u32[]{:S(2)}, u32[]{:S(2)}) async-start(bf16[4,128,2048]{2,1,0:T(8,128)(2,1)} %bitcast.173), calls=%async_computation.2 | async-start | bytes 4194304 | tf_op jit(solution)/shard_map/all_to_all | solution.py:337
  158.4 3.1 %fusion.21 = f32[512,256]{1,0:T(8,128)} fusion(bf16[64,8,2048]{2,1,0:T(8,128)(2,1)} %all-to-all-done, bf16[1,2048,256]{2,1,0:T(8,128)(2,1)S(1)} %copy-done.1), kind=kOutput, calls=%fused_computation.31 | convolution fusion | flops 536870912 | bytes 3670016 | tf_op jit(solution)/shard_map/dot_general | solution.py:268
  161.5 3.4 %fusion.17 = f32[512,256]{1,0:T(8,128)} fusion(bf16[64,8,2048]{2,1,0:T(8,128)(2,1)} %all-to-all-done, bf16[3,2048,256]{2,1,0:T(8,128)(2,1)} %copy-done.4), kind=kOutput, calls=%fused_computation.27 | convolution fusion | flops 536870912 | bytes 3670016 | tf_op jit(solution)/shard_map/dot_general | solution.py:268
  165.0 5.7 %convolution_convert_fusion.4 = bf16[512,2048]{1,0:T(8,128)(2,1)} fusion(bf16[64,8,2048]{2,1,0:T(8,128)(2,1)} %all-to-all-done, f32[512,256]{1,0:T(8,128)} %fusion.21, bf16[1,256,2048]{2,1,0:T(8,128)(2,1)} %param.26, bf16[1,2048,256]{2,1,0:T(8,128)(2,1)S(1)} %copy-done.3), kind=kOutput, calls=%fused_computation.6 | convolution fusion | flops 1075576832 | bytes 6815744 | tf_op jit(solution)/shard_map/dot_general | solution.py:327
  170.6 5.9 %convolution_convert_fusion.3 = bf16[512,2048]{1,0:T(8,128)(2,1)} fusion(bf16[256,2048]{1,0:T(8,128)(2,1)} %collective-permute-done, bf16[64,8,2048]{2,1,0:T(8,128)(2,1)} %all-to-all-done, bf16[3,2048,256]{2,1,0:T(8,128)(2,1)} %copy-done.5, f32[512,256]{1,0:T(8,128)} %fusion.17), kind=kOutput, calls=%fused_computation.5 | convolution fusion | flops 1075576832 | bytes 6815744 | tf_op jit(solution)/shard_map/dot_general | solution.py:327
  176.6 2.6 fusion.13
  179.2 2.6 fusion.9
  181.7 5.8 %convolution_convert_fusion.2 = bf16[512,2048]{1,0:T(8,128)(2,1)} fusion(bf16[256,2048]{1,0:T(8,128)(2,1)} %collective-permute-done.1, bf16[64,8,2048]{2,1,0:T(8,128)(2,1)} %all-to-all-done, bf16[3,2048,256]{2,1,0:T(8,128)(2,1)} %copy-done.5, f32[512,256]{1,0:T(8,128)S(1)} %fusion.13), kind=kOutput, calls=%fused_computation.4 | convolution fusion | flops 1075576832 | bytes 6815744 | tf_op jit(solution)/shard_map/dot_general | solution.py:327
  187.6 7.7 %fusion.1 = bf16[64,8,2048]{2,1,0:T(8,128)(2,1)} fusion(bf16[512,2048]{1,0:T(8,128)(2,1)} %convolution_convert_fusion.2, bf16[512,2048]{1,0:T(8,128)(2,1)} %convolution_convert_fusion.3, bf16[512,2048]{1,0:T(8,128)(2,1)} %convolution_convert_fusion.4, bf16[128,2048]{1,0:T(8,128)(2,1)} %collective-permute-done.3, ...), kind=kOutput, calls=%fused_computation.9 | convolution fusion | flops 1086062592 | bytes 13107200 | tf_op jit(solution)/shard_map/dot_general | solution.py:327
  195.3 5.7 %all-to-all-start.1 = ((bf16[64,8,2048]{2,1,0:T(8,128)(2,1)}), bf16[64,8,2048]{2,1,0:T(8,128)(2,1)}, u32[]{:S(2)}, u32[]{:S(2)}) async-start(bf16[64,8,2048]{2,1,0:T(8,128)(2,1)} %fusion.1), calls=%async_computation.1 | async-start | bytes 4194304 | tf_op jit(solution)/shard_map/all_to_all | solution.py:331
  201.3 0.8 copy.33
  202.1 2.1 convert_reduce_fusion
  204.2 48.0 %all-to-all-done.1 = bf16[64,8,2048]{2,1,0:T(8,128)(2,1)} async-done(((bf16[64,8,2048]{2,1,0:T(8,128)(2,1)}), bf16[64,8,2048]{2,1,0:T(8,128)(2,1)}, u32[]{:S(2)}, u32[]{:S(2)}) %all-to-all-start.1) | async-done | bytes 2097184 | tf_op jit(solution)/shard_map/all_to_all | solution.py:331
  252.2 2.1 convolution_multiply_fusion.1
  254.3 2.9 %fusion.4 = bf16[128,2048]{1,0:T(8,128)(2,1)} fusion(f32[128,2048]{1,0:T(8,128)S(1)} %convert_reduce_fusion, f32[128,2048]{1,0:T(8,128)S(1)} %convolution_multiply_fusion.1, bf16[64,8,2048]{2,1,0:T(8,128)(2,1)} %all-to-all-done.1, f32[128]{0:T(128)S(1)} %get-tuple-element.16, s32[128]{0:T(128)S(1)} %get-tuple-element.19), kind=kOutput, calls=%fused_computation.14 | convolution fusion | flops 269549568 | bytes 4719616 | tf_op jit(solution)/shard_map/dot_general | solution.py:341
  (66 shorter events, 3.7 us)
Async XLA Ops:
  7.2 138.3 %copy-start = (bf16[256,2048]{1,0:T(8,128)(2,1)S(1)}, bf16[256,2048]{1,0:T(8,128)(2,1)}, u32[]{:S(2)}) copy-start(bf16[256,2048]{1,0:T(8,128)(2,1)} %param.29) | copy-start | bytes 3145732
  7.2 134.9 %all-gather.2.cloned.1.call-start = ((), (), s32[]{:S(2)}) async-start(), calls=%async_computation.3 | async-start | bytes 2621440 | tf_op jit(solution)/shard_map/all_gather | solution.py:333
  7.2 130.3 %collective-permute-start = (bf16[256,2048]{1,0:T(8,128)(2,1)}, bf16[256,2048]{1,0:T(8,128)(2,1)}, u32[]{:S(2)}, u32[]{:S(2)}) collective-permute-start(bf16[256,2048]{1,0:T(8,128)(2,1)} %bitcast.176), channel_id=1, source_target_pairs={{0,1},{1,2},{2,3},{3,0},{4,5},{5,6},{6,7},{7,4},{8,9},{9,10},{10,1... | collective-permute-start | bytes 3145736 | tf_op jit(solution)/shard_map/ppermute | solution.py:256
  8.9 131.6 %collective-permute-start.1 = (bf16[256,2048]{1,0:T(8,128)(2,1)}, bf16[256,2048]{1,0:T(8,128)(2,1)}, u32[]{:S(2)}, u32[]{:S(2)}) collective-permute-start(bf16[256,2048]{1,0:T(8,128)(2,1)} %bitcast.177), channel_id=1, source_target_pairs={{0,3},{1,0},{2,1},{3,2},{4,7},{5,4},{6,5},{7,6},{8,11},{9,8},{10,9... | collective-permute-start | bytes 3145736 | tf_op jit(solution)/shard_map/ppermute | solution.py:257
  16.8 12.4 %copy-start.9 = (f32[64]{0:T(128)S(1)}, f32[64]{0:T(128)}, u32[]{:S(2)}) copy-start(f32[64]{0:T(128)} %param.18) | copy-start | bytes 772
  16.8 12.5 %copy-start.10 = (f32[64]{0:T(128)S(1)}, f32[64]{0:T(128)}, u32[]{:S(2)}) copy-start(f32[64]{0:T(128)} %param.19) | copy-start | bytes 772
  16.8 12.7 %copy-start.11 = (bf16[256,256]{1,0:T(8,128)(2,1)S(1)}, bf16[256,256]{1,0:T(8,128)(2,1)}, u32[]{:S(2)}) copy-start(bf16[256,256]{1,0:T(8,128)(2,1)} %param.15) | copy-start | bytes 393220
  16.8 134.3 %all-to-all-start = ((bf16[64,8,2048]{2,1,0:T(8,128)(2,1)}), bf16[64,8,2048]{2,1,0:T(8,128)(2,1)}, u32[]{:S(2)}, u32[]{:S(2)}) async-start(bf16[64,8,2048]{2,1,0:T(8,128)(2,1)} %fusion), calls=%async_computation | async-start | bytes 4194304 | tf_op jit(solution)/shard_map/all_to_all | solution.py:299
  29.1 2.1 copy-start.6
  29.1 3.2 %copy-start.7 = (bf16[256,64]{0,1:T(8,128)(2,1)S(1)}, bf16[256,64]{0,1:T(8,128)(2,1)}, u32[]{:S(2)}) copy-start(bf16[256,64]{0,1:T(8,128)(2,1)} %param.17) | copy-start | bytes 98308
  29.5 3.0 %copy-start.1 = (bf16[1,2048,256]{2,1,0:T(8,128)(2,1)S(1)}, bf16[1,2048,256]{2,1,0:T(8,128)(2,1)}, u32[]{:S(2)}) copy-start(bf16[1,2048,256]{2,1,0:T(8,128)(2,1)} %param.24) | copy-start | bytes 3145732
  32.5 1.2 copy-start.2
  134.1 1.7 copy-start.4
  135.8 1.7 copy-start.5
  138.6 49.0 %collective-permute-start.2 = (bf16[128,2048]{1,0:T(8,128)(2,1)S(1)}, bf16[128,2048]{1,0:T(8,128)(2,1)}, u32[]{:S(2)}, u32[]{:S(2)}) collective-permute-start(bf16[128,2048]{1,0:T(8,128)(2,1)S(1)} %slice.56), channel_id=1, source_target_pairs={{0,1},{1,2},{2,3},{3,0},{4,5},{5,6},{6,7},{7,4},{8,9},{9,10},{10,1... | collective-permute-start | bytes 1572872 | tf_op jit(solution)/shard_map/ppermute | solution.py:260
  141.5 46.0 %collective-permute-start.3 = (bf16[128,2048]{1,0:T(8,128)(2,1)S(1)}, bf16[128,2048]{1,0:T(8,128)(2,1)}, u32[]{:S(2)}, u32[]{:S(2)}) collective-permute-start(bf16[128,2048]{1,0:T(8,128)(2,1)S(1)} %slice.57), channel_id=1, source_target_pairs={{0,3},{1,0},{2,1},{3,2},{4,7},{5,4},{6,5},{7,6},{8,11},{9,8},{10,9... | collective-permute-start | bytes 1572872 | tf_op jit(solution)/shard_map/ppermute | solution.py:261
  151.1 44.2 %all-to-all-start.2 = ((bf16[4,128,2048]{2,1,0:T(8,128)(2,1)}), bf16[4,128,2048]{2,1,0:T(8,128)(2,1)}, u32[]{:S(2)}, u32[]{:S(2)}) async-start(bf16[4,128,2048]{2,1,0:T(8,128)(2,1)} %bitcast.173), calls=%async_computation.2 | async-start | bytes 4194304 | tf_op jit(solution)/shard_map/all_to_all | solution.py:337
  161.5 3.5 %copy-start.3 = (bf16[1,2048,256]{2,1,0:T(8,128)(2,1)S(1)}, bf16[1,2048,256]{2,1,0:T(8,128)(2,1)}, u32[]{:S(2)}) copy-start(bf16[1,2048,256]{2,1,0:T(8,128)(2,1)} %param.25) | copy-start | bytes 3145732
  195.3 5.7 %copy-start.8 = (f32[512,2]{0,1:T(2,128)S(1)}, f32[512,2]{0,1:T(2,128)}, u32[]{:S(2)}) copy-start(f32[512,2]{0,1:T(2,128)} %param.23) | copy-start | bytes 12292
  195.3 56.9 %all-to-all-start.1 = ((bf16[64,8,2048]{2,1,0:T(8,128)(2,1)}), bf16[64,8,2048]{2,1,0:T(8,128)(2,1)}, u32[]{:S(2)}, u32[]{:S(2)}) async-start(bf16[64,8,2048]{2,1,0:T(8,128)(2,1)} %fusion.1), calls=%async_computation.1 | async-start | bytes 4194304 | tf_op jit(solution)/shard_map/all_to_all | solution.py:331
Sparse Core Ops, SparseCore 0:
  13.0 46.8 all-gather.1

commit v3 on v2

v3 whole, which is shorter than its diff:
```python
import functools

import jax
import jax.numpy as jnp
from jax import lax
from jax.experimental import pallas as pl
from jax.experimental.pallas import tpu as pltpu
from jax.sharding import Mesh
from jax.sharding import PartitionSpec as P

GRID_W = 64
EP = ("ep_0", "ep_1", "ep_2")
EP_TP = ("ep_0", "ep_1", "ep_2", "tp")
MESH_ID = pl.DeviceIdType.MESH
Z, X, CORE, Y = EP_TP


epsilon = 1e-06
rotary_base = 10000.0
routed_scale = 2.5


def lane_places(heads, size, offset):
    source = jnp.arange(heads * size)[None, :, None]
    lane = jnp.arange(128)[None, None, :] - offset
    head = jnp.arange(heads)[:, None, None]
    inside = (lane >= 0) & (lane < size)
    straight = inside & (source == head * size + lane)
    swapped = inside & (source == head * size + (lane ^ 1))
    return straight.astype(jnp.bfloat16), swapped.astype(jnp.bfloat16)


def rotated(rows_in, gain, heads, size, positions):
    straight, swapped = lane_places(heads, size, 0)
    own = jnp.einsum("td,hde->hte", rows_in, straight, preferred_element_type=jnp.float32)
    other = jnp.einsum("td,hde->hte", rows_in, swapped, preferred_element_type=jnp.float32)
    lane = jnp.arange(128)
    wide = jnp.pad(gain, (0, 128 - size))
    wide_swapped = jnp.pad(gain.reshape(-1, 2)[:, ::-1].reshape(-1), (0, 128 - size))
    factor = lax.rsqrt(jnp.sum(own * own, axis=-1, keepdims=True) / size + epsilon)
    pair_count = size // 4
    pair = (lane // 2) % (2 * pair_count)
    inv_freq = rotary_base ** (-(pair % pair_count).astype(jnp.float32) / pair_count)
    grid_row = (positions // GRID_W).astype(jnp.float32)[:, None]
    grid_col = (positions % GRID_W).astype(jnp.float32)[:, None]
    angles = jnp.where(pair[None, :] < pair_count, grid_row, grid_col) * inv_freq[None, :]
    sign = jnp.where(lane % 2 == 0, -1.0, 1.0)
    turned = (own * factor * wide) * jnp.cos(angles) + (other * factor * wide_swapped) * (
        sign * jnp.sin(angles)
    )
    return turned.astype(jnp.bfloat16)


def token_slots(own_routes, capacity):
    rows = own_routes.shape[0]
    earlier = jnp.arange(rows)[:, None] < jnp.arange(rows)[None, :]
    slots = []
    for k in range(own_routes.shape[1]):
        mine = own_routes[:, k]
        same = own_routes[:, 0][:, None] == mine[None, :]
        for other in range(1, own_routes.shape[1]):
            same = same | (own_routes[:, other][:, None] == mine[None, :])
        rank = jnp.sum((same & earlier).astype(jnp.int32), axis=0)
        slots.append(mine * capacity + rank)
    return slots


CHUNKS = 4
TILE = 256


def layer_kernel(
    q_ref, kv_ref, send_ref, normed_ref, pick_ref, scale_ref,
    gate_ref, up_ref, down_ref, shared_gate_ref, shared_up_ref, shared_down_ref,
    attn_ref, moe_ref,
    buf, run_max, run_sum, mixed,
    w_gate, w_up, w_down, s_gate, s_up, s_down,
    arrived, rows, hidden, out, returned,
    group, part, part_in, relay,
    z_send, z_recv, x_send, x_recv, c_send, c_recv, w_send, w_recv, d_send, d_recv,
    disp_send, disp_recv, ret_send, ret_recv, g_send, g_recv, p_send, p_recv, own_sem,
):
    z, x, core, y = (lax.axis_index(name) for name in EP_TP)
    z_size, x_size, cores, y_size = buf.shape[2], buf.shape[1], buf.shape[0], 4
    experts, capacity = arrived.shape[0], arrived.shape[1]
    model_width = normed_ref.shape[1]
    tokens = normed_ref.shape[0]
    width = model_width // CHUNKS
    me = (z * x_size + x) * cores + core

    def near(index, step, size):
        return lax.rem(index + step + size, size)

    def member(index):
        return {
            Z: index // (x_size * cores),
            X: lax.rem(index // cores, x_size),
            CORE: lax.rem(index, cores),
        }

    def remote(src, dst, send_sem, recv_sem, peer):
        return pltpu.make_async_remote_copy(
            src_ref=src, dst_ref=dst, send_sem=send_sem, recv_sem=recv_sem,
            device_id=peer, device_id_type=MESH_ID,
        )

    x_right, x_left, x_far = near(x, 1, x_size), near(x, -1, x_size), near(x, 2, x_size)
    right, left = {Y: near(y, 1, y_size)}, {Y: near(y, -1, y_size)}
    barrier = pltpu.get_barrier_semaphore()

    def greet(k, carry):
        pl.semaphore_signal(
            barrier, inc=1, device_id=member(lax.rem(me + k, experts)), device_id_type=MESH_ID
        )
        return carry

    lax.fori_loop(1, experts, greet, 0)
    for peer in (right, left):
        pl.semaphore_signal(barrier, inc=1, device_id=peer, device_id_type=MESH_ID)
    pl.semaphore_wait(barrier, experts + 1)

    def ring_copies(slots, own_source, pick, size, send_sems, recv_sems):
        first, second = pl.ds(0, size // 2), pl.ds(size // 2, size // 2)
        return (
            remote(own_source, pick(slots, 1), send_sems.at[0], recv_sems.at[0], right),
            remote(own_source, pick(slots, 2), send_sems.at[1], recv_sems.at[1], left),
            remote(
                pick(slots, 1, first), pick(slots, 3, first), send_sems.at[2], recv_sems.at[2], right
            ),
            remote(
                pick(slots, 2, second), pick(slots, 3, second), send_sems.at[3], recv_sems.at[3], left
            ),
        )

    def whole(slots, slot, span=None):
        return slots.at[slot] if span is None else slots.at[slot, span]

    depth = gate_ref.shape[0]
    gates = ring_copies(w_gate, gate_ref, whole, depth, w_send.at[0], w_recv.at[0])
    ups = ring_copies(w_up, up_ref, whole, depth, w_send.at[1], w_recv.at[1])
    downs = []
    units = down_ref.shape[0]
    for n in range(CHUNKS):
        columns = pl.ds(n * width, width)

        def some(slots, slot, span=None, columns=columns):
            return slots.at[slot, pl.ds(0, units) if span is None else span, columns]

        downs.append(
            ring_copies(
                w_down, down_ref.at[:, columns], some, units, d_send.at[n], d_recv.at[n]
            )
        )

    def start_both(ring):
        ring[0].start()
        ring[1].start()

    def pass_on(ring):
        ring[0].wait_recv()
        ring[2].start()
        ring[1].wait_recv()
        ring[3].start()

    def far_arrived(ring):
        ring[2].wait_recv()
        ring[3].wait_recv()

    start_both(gates)
    start_both(ups)

    along_z = [
        remote(kv_ref, buf.at[core, x, z], z_send.at[k], z_recv.at[k], {Z: near(z, k, z_size)})
        for k in range(1, z_size)
    ]
    for copy in along_z:
        copy.start()

    def send_rows(i, carry):
        to = lax.rem(me + lax.rem(i * 13, experts), experts)
        remote(send_ref.at[to], arrived.at[me], disp_send, disp_recv, member(to)).start()
        return carry

    lax.fori_loop(1, experts, send_rows, 0)
    locals_ = [
        pltpu.make_async_copy(source, target, own_sem.at[n])
        for n, (source, target) in enumerate((
            (kv_ref, buf.at[core, x, z]),
            (send_ref.at[me], arrived.at[me]),
            (gate_ref, w_gate.at[0]),
            (up_ref, w_up.at[0]),
            (down_ref, w_down.at[0]),
            (shared_gate_ref, s_gate),
            (shared_up_ref, s_up),
            (shared_down_ref, s_down),
            (normed_ref, group.at[0]),
        ))
    ]
    for copy in locals_:
        copy.start()
    run_max[...] = jnp.full_like(run_max, -jnp.inf)
    run_sum[...] = jnp.zeros_like(run_sum)
    mixed[...] = jnp.zeros_like(mixed)
    locals_[0].wait()
    for copy in along_z:
        copy.wait_recv()

    def attend(which_core, which_x):
        keys = buf.shape[2] * buf.shape[3]

        def tile(i, carry):
            here = pl.ds(i * TILE, TILE)
            span = buf[which_core, which_x].reshape(keys, 128)
            scores = lax.dot_general(
                q_ref[here, :], span, (((1,), (1,)), ((), ())), preferred_element_type=jnp.float32
            )
            old_max = run_max[here, :]
            new_max = jnp.maximum(old_max, jnp.max(scores, axis=1, keepdims=True))
            factor = jnp.exp(old_max - new_max)
            weights_now = jnp.exp(scores - new_max[:, :1])
            run_sum[here, :] = run_sum[here, :] * factor + jnp.sum(
                weights_now, axis=1, keepdims=True
            )
            mixed[here, :] = mixed[here, :] * factor + jnp.dot(
                weights_now.astype(jnp.bfloat16), span, preferred_element_type=jnp.float32
            )
            run_max[here, :] = new_max
            return carry

        lax.fori_loop(0, q_ref.shape[0] // TILE, tile, 0)

    def line_to_core(which_x, slot):
        return remote(
            buf.at[core, which_x], buf.at[core, which_x], c_send.at[slot], c_recv.at[slot],
            {CORE: 1 - core},
        )

    line = buf.at[core, x]
    to_right = remote(line, line, x_send.at[0], x_recv.at[0], {X: x_right})
    to_left = remote(line, line, x_send.at[1], x_recv.at[1], {X: x_left})
    first, second = pl.ds(0, z_size // 2), pl.ds(z_size // 2, z_size // 2)
    on_right = remote(
        buf.at[core, x_left, first], buf.at[core, x_left, first],
        x_send.at[2], x_recv.at[2], {X: x_right},
    )
    on_left = remote(
        buf.at[core, x_right, second], buf.at[core, x_right, second],
        x_send.at[3], x_recv.at[3], {X: x_left},
    )
    lines = [line_to_core(which, n) for n, which in enumerate((x, x_left, x_right, x_far))]
    to_right.start()
    to_left.start()
    lines[0].start()
    attend(core, x)
    lines[0].wait_recv()
    attend(1 - core, x)
    to_right.wait_recv()
    on_right.start()
    lines[1].start()
    to_left.wait_recv()
    on_left.start()
    lines[2].start()
    pass_on(gates)
    attend(core, x_left)
    attend(core, x_right)
    on_right.wait_recv()
    on_left.wait_recv()
    lines[3].start()
    lines[1].wait_recv()
    pass_on(ups)
    for n in range(CHUNKS):
        start_both(downs[n])
    attend(1 - core, x_left)
    lines[2].wait_recv()
    attend(1 - core, x_right)
    attend(core, x_far)
    lines[3].wait_recv()
    attend(1 - core, x_far)
    attn_ref[...] = (mixed[...] / run_sum[...]).astype(attn_ref.dtype)

    others = pl.ds(0, experts - 1)
    pltpu.make_async_copy(arrived.at[others], arrived.at[others], disp_recv).wait()
    for copy in locals_[1:]:
        copy.wait()

    def flatten(i, carry):
        block = arrived[pl.ds(i * 8, 8)].astype(jnp.float32).reshape(8 * capacity, model_width)
        rows[pl.ds(i * 8 * capacity, 8 * capacity), :] = block.astype(jnp.bfloat16)
        return carry

    lax.fori_loop(0, experts // 8, flatten, 0)

    def activated(source, gate_now, up_now):
        gate_proj = jnp.dot(source, gate_now, preferred_element_type=jnp.float32)
        up_proj = jnp.dot(source, up_now, preferred_element_type=jnp.float32)
        return (gate_proj / (1.0 + jnp.exp(-gate_proj)) * up_proj).astype(jnp.bfloat16)

    def fill_hidden(slot):
        def tile(i, carry):
            here = pl.ds(i * TILE, TILE)
            hidden[here, slot * units : (slot + 1) * units] = activated(
                rows[here, :], w_gate[slot], w_up[slot]
            )
            return carry

        lax.fori_loop(0, rows.shape[0] // TILE, tile, 0)

    for slot in range(3):
        fill_hidden(slot)
    pass_on(downs[0])
    far_arrived(gates)
    far_arrived(ups)
    fill_hidden(3)
    shared_ring = ring_copies(group, normed_ref, whole, tokens, g_send, g_recv)
    for n in range(CHUNKS):
        if n + 1 < CHUNKS:
            pass_on(downs[n + 1])
        else:
            start_both(shared_ring)
        far_arrived(downs[n])

        def product(i, carry, n=n):
            here = pl.ds(i * TILE, TILE)
            value = jnp.dot(
                hidden[here, :],
                w_down[:, :, n * width : (n + 1) * width].reshape(4 * units, width),
                preferred_element_type=jnp.float32,
            )
            count = TILE // capacity
            out[n, pl.ds(i * count, count)] = value.reshape(count, capacity, width).astype(
                jnp.bfloat16
            )
            return carry

        lax.fori_loop(0, rows.shape[0] // TILE, product, 0)

        def send_back(i, carry, n=n):
            to = lax.rem(me + lax.rem(i * 13, experts), experts)
            remote(
                out.at[n, to], returned.at[n, me], ret_send.at[n], ret_recv.at[n], member(to)
            ).start()
            return carry

        lax.fori_loop(1, experts, send_back, 0)
        pltpu.make_async_copy(out.at[n, me], returned.at[n, me], own_sem.at[9 + n]).start()

    pass_on(shared_ring)

    def shared_part(slot):
        value = activated(group[slot], s_gate[...], s_up[...])
        for n in range(CHUNKS):
            columns = slice(n * width, (n + 1) * width)
            part[slot, :, columns] = jnp.dot(
                value, s_down[:, columns], preferred_element_type=jnp.float32
            ).astype(jnp.bfloat16)

    top, bottom = pl.ds(0, tokens // 2), pl.ds(tokens // 2, tokens // 2)
    part_left = remote(part.at[1], part_in.at[2], p_send.at[0], p_recv.at[0], left)
    part_right = remote(part.at[2], part_in.at[1], p_send.at[1], p_recv.at[1], right)
    via_right = remote(part.at[3, top], relay.at[0], p_send.at[2], p_recv.at[2], right)
    via_left = remote(part.at[3, bottom], relay.at[1], p_send.at[3], p_recv.at[3], left)
    on_to_right = remote(relay.at[0], part_in.at[0, top], p_send.at[4], p_recv.at[4], right)
    on_to_left = remote(relay.at[1], part_in.at[0, bottom], p_send.at[5], p_recv.at[5], left)
    shared_part(1)
    part_left.start()
    shared_part(2)
    part_right.start()
    far_arrived(shared_ring)
    shared_part(3)
    via_right.start()
    via_left.start()
    shared_part(0)
    via_right.wait_recv()
    on_to_right.start()
    via_left.wait_recv()
    on_to_left.start()
    part_left.wait_recv()
    part_right.wait_recv()
    on_to_right.wait_recv()
    on_to_left.wait_recv()

    for n in range(CHUNKS):
        pltpu.make_async_copy(
            returned.at[n, others], returned.at[n, others], ret_recv.at[n]
        ).wait()
        pltpu.make_async_copy(out.at[n, me], returned.at[n, me], own_sem.at[9 + n]).wait()
        columns = slice(n * width, (n + 1) * width)
        results = returned[n].astype(jnp.float32).reshape(experts * capacity, width)
        results = results.astype(jnp.bfloat16)
        total = part[0, :, columns].astype(jnp.float32)
        for slot in range(3):
            total = total + part_in[slot, :, columns].astype(jnp.float32)
        routed = None
        for k in range(pick_ref.shape[0]):
            picked = jnp.dot(pick_ref[k], results, preferred_element_type=jnp.float32)
            term = scale_ref[k][:, :1] * picked
            routed = term if routed is None else routed + term
        moe_ref[:, columns] = (routed + total).astype(moe_ref.dtype)

    for ring in [gates, ups, shared_ring] + downs:
        for copy in ring:
            copy.wait_send()
    for copy in along_z + [to_right, to_left, on_right, on_left] + lines:
        copy.wait_send()
    for copy in (part_left, part_right, via_right, via_left, on_to_right, on_to_left):
        copy.wait_send()
    pltpu.make_async_copy(send_ref.at[others], arrived.at[others], disp_send).wait()
    for n in range(CHUNKS):
        pltpu.make_async_copy(out.at[n, others], returned.at[n, others], ret_send.at[n]).wait()


def run_layer(q_rows, key_value, send, normed, picks, scales, expert_weights, shared_weights):
    query_count = q_rows.shape[0]
    tokens = key_value.shape[0]
    z_size, x_size, cores = (lax.axis_size(name) for name in EP)
    experts, capacity, model_width = send.shape
    depth, units = expert_weights[0].shape
    rows, own = experts * capacity, normed.shape[0]
    dma = pltpu.SemaphoreType.DMA
    bf16, f32 = jnp.bfloat16, jnp.float32
    width = model_width // CHUNKS
    vmem, anywhere = pl.BlockSpec(memory_space=pltpu.VMEM), pl.BlockSpec(memory_space=pl.ANY)
    keys = tokens * z_size * x_size * cores
    return pl.pallas_call(
        layer_kernel,
        out_shape=[
            jax.ShapeDtypeStruct((query_count, 128), bf16),
            jax.ShapeDtypeStruct(normed.shape, bf16),
        ],
        in_specs=[vmem, vmem, anywhere, vmem, vmem, vmem] + [anywhere] * 6,
        out_specs=[vmem, vmem],
        scratch_shapes=[
            pltpu.VMEM((cores, x_size, z_size, tokens, 128), bf16),
            pltpu.VMEM((query_count, 128), f32),
            pltpu.VMEM((query_count, 128), f32),
            pltpu.VMEM((query_count, 128), f32),
            pltpu.VMEM((4, depth, units), bf16),
            pltpu.VMEM((4, depth, units), bf16),
            pltpu.VMEM((4, units, depth), bf16),
            pltpu.VMEM((depth, units), bf16),
            pltpu.VMEM((depth, units), bf16),
            pltpu.VMEM((units, depth), bf16),
            pltpu.VMEM((experts, capacity, model_width), bf16),
            pltpu.VMEM((rows, model_width), bf16),
            pltpu.VMEM((rows, 4 * units), bf16),
            pltpu.VMEM((CHUNKS, experts, capacity, width), bf16),
            pltpu.VMEM((CHUNKS, experts, capacity, width), bf16),
            pltpu.VMEM((4, own, model_width), bf16),
            pltpu.VMEM((4, own, model_width), bf16),
            pltpu.VMEM((3, own, model_width), bf16),
            pltpu.VMEM((2, own // 2, model_width), bf16),
            dma((z_size,)), dma((z_size,)),
            dma((4,)), dma((4,)),
            dma((4,)), dma((4,)),
            dma((2, 4)), dma((2, 4)),
            dma((CHUNKS, 4)), dma((CHUNKS, 4)),
            dma, dma,
            dma((CHUNKS,)), dma((CHUNKS,)),
            dma((4,)), dma((4,)),
            dma((6,)), dma((6,)),
            dma((9 + CHUNKS,)),
        ],
        compiler_params=pltpu.CompilerParams(
            collective_id=0, has_side_effects=True, vmem_limit_bytes=60 * 1024 * 1024
        ),
        cost_estimate=pl.CostEstimate(
            flops=60 * query_count * keys * 128 // 2, bytes_accessed=2 * keys * 256, transcendentals=0
        ),
        name="layer",
    )(q_rows, key_value, send, normed, picks, scales, *expert_weights, *shared_weights)


def dispatch(moe_tokens, norm_gain, routes, route_weights):
    tok_rows, model_width = moe_tokens.shape
    top_count = routes.shape[1]
    experts = lax.axis_size(EP)
    capacity = 2 * tok_rows * top_count // experts
    lane = lax.axis_index("tp")
    values32 = moe_tokens.astype(jnp.float32)
    normed = (
        values32
        * lax.rsqrt(jnp.mean(values32 * values32, axis=-1, keepdims=True) + epsilon)
        * norm_gain
    ).astype(jnp.bfloat16)
    own_routes = lax.dynamic_slice_in_dim(routes, lane * tok_rows, tok_rows, 0)
    own_weights = lax.dynamic_slice_in_dim(route_weights, lane * tok_rows, tok_rows, 0)
    gates = own_weights / jnp.sum(own_weights, axis=-1, keepdims=True) * routed_scale
    slots = token_slots(own_routes, capacity)
    places = jnp.arange(experts * capacity, dtype=jnp.int32)
    placed = (places[:, None] == slots[0][None, :]) | (places[:, None] == slots[1][None, :])
    send = jnp.dot(placed.astype(jnp.bfloat16), normed, preferred_element_type=jnp.float32)
    send = send.astype(jnp.bfloat16).reshape(experts, capacity, model_width)
    picks = jnp.stack([(slot[:, None] == places[None, :]).astype(jnp.bfloat16) for slot in slots])
    scales = jnp.broadcast_to(gates.T[:, :, None], (top_count, tok_rows, 128))
    return send, normed, picks, scales


def body(
    query_rows,
    key_rows,
    value_rows,
    query_gain,
    key_gain,
    moe_tokens,
    norm_gain,
    routes,
    route_weights,
    expert_gate,
    expert_up,
    expert_down,
    shared_gate,
    shared_up,
    shared_down,
):
    dispatched = dispatch(moe_tokens, norm_gain, routes, route_weights)
    row_count = query_rows.shape[0]
    size = query_gain.shape[0]
    heads = query_rows.shape[1] // size
    positions = lax.axis_index(EP) * row_count + jnp.arange(row_count, dtype=jnp.int32)
    q_rot = rotated(query_rows, query_gain, heads, size, positions) * jnp.bfloat16(size**-0.5)
    k_rot = rotated(key_rows, key_gain, 1, size, positions)[0]
    placed = lane_places(1, size, size)[0][0]
    values = jnp.dot(value_rows, placed, preferred_element_type=jnp.float32).astype(jnp.bfloat16)
    attn, moe_out = run_layer(
        q_rot.reshape(heads * row_count, 128),
        k_rot + values,
        *dispatched,
        (expert_gate[0], expert_up[0], expert_down[0]),
        (shared_gate, shared_up, shared_down),
    )
    attn_out = attn[:, size:].reshape(heads, row_count, size).transpose(1, 0, 2)
    return (attn_out.reshape(row_count, heads * size), moe_out)


def solution(mesh):
    finer = Mesh(mesh.devices.reshape(8, 4, 2, mesh.shape["tp"]), ("ep_0", "ep_1", "ep_2", "tp"))
    return jax.shard_map(
        body,
        mesh=finer,
        in_specs=(
            P(EP, "tp"),
            P(EP, "tp"),
            P(EP, "tp"),
            P(),
            P(),
            P(EP_TP, None),
            P(),
            P(EP, None),
            P(EP, None),
            P(EP, None, "tp"),
            P(EP, None, "tp"),
            P(EP, "tp", None),
            P(None, "tp"),
            P(None, "tp"),
            P("tp", None),
        ),
        out_specs=(P(EP, "tp"), P(EP_TP, None)),
        check_vma=False,
    )
```

time: 265 us -> 185 us (0.70)
  Pallas kernels: 100 us -> 163 us
  matrix products: 55.7 us -> 5.96 us
  waiting for transfers between devices: 48 us -> 0 us
  starting transfers between devices: 30.1 us -> 0 us
  between operations: 14.4 us -> 0.89 us
    pallas_call x1, Pallas kernels: 100 us -> 163 us  [run_layer(): pl.pallas_call(layer_kernel, out_shape=[jax.ShapeDtypeStruct((query_count...]
    dot_general x13 -> x1, matrix products: 54 us -> 2.05 us  [dispatch(): jnp.dot(placed.astype(jnp.bfloat16), normed, preferred_element_type=jnp.f...]
    all_to_all x3 -> x0, waiting for transfers between devices: 48 us -> none  [the longest x1 48 us: experts_half(): lax.all_to_all(outgoing, EP, split_axis=0, concat_axis=0, tiled=True)]
    all_to_all x3 -> x0, starting transfers between devices: 25.3 us -> none  [the longest x1 12.3 us: dispatch(): lax.all_to_all(send.reshape(experts, capacity, model_width), EP, split_ax...]
    ppermute x4 -> x0, starting transfers between devices: 4.73 us -> none  [the longest x1 1.88 us: from_ring(): lax.ppermute(left[:half], 'tp', ring(1))]
    unnamed x25 -> x12, local copies, waits for them, and re-layouts: 5.36 us -> 2.67 us
  transfers between devices with their start and end apart: 8 -> 0, of which waited for: 1 -> 0; matrix products, arithmetic and copies ran while one was open for 23% -> 0% of each run, Pallas kernels for 38% -> 0%
where the time goes in v3:
time: 185 us; the launch traced here: 184 us
  Pallas kernels  163 us (88%)
  local copies, waits for them, and re-layouts  9.43 us (5%)
  matrix products  5.96 us (3%)
  other arithmetic  4.53 us (2%)
    pallas_call x1, Pallas kernels, run_layer(): pl.pallas_call(layer_kernel, out_shape=[jax.ShapeDtypeStruct((query_count...  163 us

profile of v3, /device:TPU:8, one launch (start us, length us, event | category | flops | bytes accessed | tf_op | source)
XLA Modules:
  0.0 184.1 jit_solution(13564821002032839431)
XLA Ops:
  0.6 0.0 copy-start
  0.7 0.7 pad.13
  1.4 0.7 pad.15
  2.1 1.2 fusion.16
  3.3 0.7 dynamic-slice_reduce_fusion
  4.0 0.7 multiply_bitcast_fusion
  4.7 0.7 constant_dynamic-slice_fusion
  5.4 0.1 convert_reduce_fusion.1
  5.6 0.1 broadcast_add_fusion
  5.7 0.7 reshape.650
  6.4 0.1 rev.6
  6.5 0.1 reshape.651
  6.6 0.8 reshape.653
  7.4 0.1 rev.7
  7.5 0.1 reshape.654
  7.6 0.8 broadcast_in_dim.59.scale_ref
  8.3 0.1 iota_compare_fusion.2
  8.5 0.8 add_convert_fusion.pick_ref
  9.2 1.0 multiply_reduce_fusion.1
  10.3 1.4 fusion.15
  11.7 0.8 fusion.14.kv_ref
  12.5 0.6 fusion.34
  13.1 0.2 fusion.18.normed_ref
  13.4 0.3 multiply_reduce_fusion
  13.7 0.3 fusion.6
  14.0 0.9 copy.28
  14.9 2.0 %fusion.send_ref = bf16[64,8,2048]{2,1,0:T(8,128)(2,1)} fusion(bf16[128,2048]{1,0:T(8,128)(2,1)S(1)} %fusion.18.normed_ref, s32[128]{0:T(128)S(1)} %get-tuple-element.17, s32[128]{0:T(128)S(1)} %get-tuple-element.16), kind=kOutput, calls=%fused_computation.1 | convolution fusion | flops 269680640 | bytes 2622464 | tf_op jit(solution)/shard_map/dot_general | solution.py:491
  16.9 163.3 %layer.1 = (bf16[1024,128]{1,0:T(8,128)(2,1)}, bf16[128,2048]{1,0:T(8,128)(2,1)}) custom-call(bf16[1024,128]{1,0:T(8,128)(2,1)} %bitcast.97, bf16[256,128]{1,0:T(8,128)(2,1)} %fusion.14.kv_ref, bf16[64,8,2048]{2,1,0:T(8,128)(2,1)} %fusion.send_ref, bf16[128,2048]{1,0:T(8,128)(2,1)} %copy-done.1, bf16[2,128,512]{2,1,0:T(8,128)(2,1)} %add_convert_fusion.pick_ref, ...), custom_call_target="tpu_custom_call" | custom-call | flops 64424509440 | bytes 8388608 | tf_op jit(solution)/shard_map/layer/pallas_call | solution.py:424
  180.2 1.1 slice.15
  181.3 0.1 copy.32
  181.4 0.8 copy.33
  182.2 1.9 %copy.38 = bf16[128,2048]{1,0:T(8,128)(2,1)} copy(bf16[128,2048]{1,0:T(8,128)(2,1)} %get-tuple-element.37) | data formatting | bytes 1048576
  (24 shorter events, 0.1 us)
Async XLA Ops:
  0.6 12.7 %copy-start = (bf16[256,256]{1,0:T(8,128)(2,1)S(1)}, bf16[256,256]{1,0:T(8,128)(2,1)}, u32[]{:S(2)}) copy-start(bf16[256,256]{1,0:T(8,128)(2,1)} %param.15) | copy-start | bytes 393220
  0.6 12.5 %copy-start.2 = (bf16[128,2048]{1,0:T(8,128)(2,1)S(1)}, bf16[128,2048]{1,0:T(8,128)(2,1)}, u32[]{:S(2)}) copy-start(bf16[128,2048]{1,0:T(8,128)(2,1)} %param.20) | copy-start | bytes 1572868
  0.7 12.5 %copy-start.4 = (f32[2048]{0:T(1024)S(1)}, f32[2048]{0:T(1024)}, u32[]{:S(2)}) copy-start(f32[2048]{0:T(1024)} %param.21) | copy-start | bytes 24580
  0.7 11.0 %copy-start.3 = (bf16[256,64]{0,1:T(8,128)(2,1)S(1)}, bf16[256,64]{0,1:T(8,128)(2,1)}, u32[]{:S(2)}) copy-start(bf16[256,64]{0,1:T(8,128)(2,1)} %param.17) | copy-start | bytes 98308
  13.3 3.6 %copy-start.1 = (bf16[128,2048]{1,0:T(8,128)(2,1)}, bf16[128,2048]{1,0:T(8,128)(2,1)S(1)}, u32[]{:S(2)}) copy-start(bf16[128,2048]{1,0:T(8,128)(2,1)S(1)} %fusion.18.normed_ref) | copy-start | bytes 1572868

commit v4 on v3

--- a/solution.py
+++ b/solution.py
@@ -51,6 +51,10 @@
     return turned.astype(jnp.bfloat16)
 
 
+def ring(step):
+    return [(i, (i + step) % 4) for i in range(4)]
+
+
 def token_slots(own_routes, capacity):
     rows = own_routes.shape[0]
     earlier = jnp.arange(rows)[:, None] < jnp.arange(rows)[None, :]
@@ -71,14 +75,16 @@
 
 def layer_kernel(
     q_ref, kv_ref, send_ref, normed_ref, pick_ref, scale_ref,
+    gate_left_ref, gate_right_ref,
     gate_ref, up_ref, down_ref, shared_gate_ref, shared_up_ref, shared_down_ref,
     attn_ref, moe_ref,
     buf, run_max, run_sum, mixed,
     w_gate, w_up, w_down, s_gate, s_up, s_down,
     arrived, rows, hidden, out, returned,
-    group, part, part_in, relay,
+    shared_sum, row_relay, result_relay,
     z_send, z_recv, x_send, x_recv, c_send, c_recv, w_send, w_recv, d_send, d_recv,
-    disp_send, disp_recv, ret_send, ret_recv, g_send, g_recv, p_send, p_recv, own_sem,
+    disp_send, disp_recv, ret_send, ret_recv, sy_send, sy_recv, sx_send, sx_recv, sc_send, sc_recv,
+    relay_send, relay_recv, own_sem,
 ):
     z, x, core, y = (lax.axis_index(name) for name in EP_TP)
     z_size, x_size, cores, y_size = buf.shape[2], buf.shape[1], buf.shape[0], 4
@@ -136,7 +142,15 @@
         return slots.at[slot] if span is None else slots.at[slot, span]
 
     depth = gate_ref.shape[0]
-    gates = ring_copies(w_gate, gate_ref, whole, depth, w_send.at[0], w_recv.at[0])
+    early, late = pl.ds(0, depth // 2), pl.ds(depth // 2, depth // 2)
+    gates = (
+        remote(gate_ref.at[late], w_gate.at[1, late], w_send.at[0, 0], w_recv.at[0, 0], right),
+        remote(gate_ref.at[late], w_gate.at[2, late], w_send.at[0, 1], w_recv.at[0, 1], left),
+        remote(gate_left_ref, w_gate.at[3, early], w_send.at[0, 2], w_recv.at[0, 2], right),
+        remote(
+            w_gate.at[2, late], w_gate.at[3, late], w_send.at[0, 3], w_recv.at[0, 3], left
+        ),
+    )
     ups = ring_copies(w_up, up_ref, whole, depth, w_send.at[1], w_recv.at[1])
     downs = []
     units = down_ref.shape[0]
@@ -166,22 +180,95 @@
         ring[2].wait_recv()
         ring[3].wait_recv()
 
-    start_both(gates)
-    start_both(ups)
-
+    shared = (
+        (shared_gate_ref, s_gate, s_gate.shape[1] // (x_size * cores)),
+        (shared_up_ref, s_up, s_up.shape[1] // (x_size * cores)),
+        (shared_down_ref, s_down, s_down.shape[1] // (x_size * cores)),
+    )
+
+    def share(which_x, size, part=None):
+        start = (which_x * cores + core) * size
+        if part is None:
+            return pl.ds(pl.multiple_of(start, size), size)
+        return pl.ds(pl.multiple_of(start + part * (size // 2), size // 2), size // 2)
+
+    got = pl.ds(1, 3)
+    over_y, over_x, over_cores = [], [], []
+    for n, (source, slots, size) in enumerate(shared):
+        mine = share(x, size)
+        over_y.append((
+            remote(source.at[mine], slots.at[1, mine], sy_send.at[n, 0], sy_recv.at[n, 0], right),
+            remote(source.at[mine], slots.at[2, mine], sy_send.at[n, 1], sy_recv.at[n, 1], left),
+            remote(
+                slots.at[1, share(x, size, 0)], slots.at[3, share(x, size, 0)],
+                sy_send.at[n, 2], sy_recv.at[n, 2], right,
+            ),
+            remote(
+                slots.at[2, share(x, size, 1)], slots.at[3, share(x, size, 1)],
+                sy_send.at[n, 3], sy_recv.at[n, 3], left,
+            ),
+        ))
+        from_left, from_right = share(x_left, size, 0), share(x_right, size, 1)
+        over_x.append((
+            remote(
+                slots.at[got, mine], slots.at[got, mine],
+                sx_send.at[n, 0], sx_recv.at[n, 0], {X: x_right},
+            ),
+            remote(
+                slots.at[got, mine], slots.at[got, mine],
+                sx_send.at[n, 1], sx_recv.at[n, 1], {X: x_left},
+            ),
+            remote(
+                slots.at[got, from_left], slots.at[got, from_left],
+                sx_send.at[n, 2], sx_recv.at[n, 2], {X: x_right},
+            ),
+            remote(
+                slots.at[got, from_right], slots.at[got, from_right],
+                sx_send.at[n, 3], sx_recv.at[n, 3], {X: x_left},
+            ),
+        ))
+        over_cores.append([
+            remote(
+                slots.at[got, share(which, size)], slots.at[got, share(which, size)],
+                sc_send.at[n, k], sc_recv.at[n, k], {CORE: 1 - core},
+            )
+            for k, which in enumerate((x, x_left, x_right, x_far))
+        ])
+
+    for ring in over_y:
+        start_both(ring)
+    gates[2].start()
+
+    blocks = x_size * cores
+    relayed = blocks // 2
+    z_far, z_below, z_source = near(z, z_size // 2, z_size), near(z, -1, z_size), near(z, 1, z_size)
+    relay_target = near(z, -(z_size // 2 - 1), z_size)
+    relay_origin = (z_source * x_size + x) * cores + core
+    far_blocks = pl.ds(z_far * blocks, relayed)
+
+    def spread(send_one):
+        def step(i, carry):
+            to = lax.rem(me + lax.rem(i * 13, experts), experts)
+            by_relay = jnp.logical_and(to // blocks == z_far, lax.rem(to, blocks) < relayed)
+
+            @pl.when(jnp.logical_not(by_relay))
+            def _():
+                send_one(to)
+
+            return carry
+
+        lax.fori_loop(1, experts, step, 0)
+
+    row_hop = remote(
+        send_ref.at[far_blocks], row_relay, relay_send.at[0], relay_recv.at[0], {Z: z_below}
+    )
+    row_hop.start()
     along_z = [
         remote(kv_ref, buf.at[core, x, z], z_send.at[k], z_recv.at[k], {Z: near(z, k, z_size)})
         for k in range(1, z_size)
     ]
     for copy in along_z:
         copy.start()
-
-    def send_rows(i, carry):
-        to = lax.rem(me + lax.rem(i * 13, experts), experts)
-        remote(send_ref.at[to], arrived.at[me], disp_send, disp_recv, member(to)).start()
-        return carry
-
-    lax.fori_loop(1, experts, send_rows, 0)
     locals_ = [
         pltpu.make_async_copy(source, target, own_sem.at[n])
         for n, (source, target) in enumerate((
@@ -190,10 +277,11 @@
             (gate_ref, w_gate.at[0]),
             (up_ref, w_up.at[0]),
             (down_ref, w_down.at[0]),
-            (shared_gate_ref, s_gate),
-            (shared_up_ref, s_up),
-            (shared_down_ref, s_down),
-            (normed_ref, group.at[0]),
+            (shared_gate_ref, s_gate.at[0]),
+            (shared_up_ref, s_up.at[0]),
+            (shared_down_ref, s_down.at[0]),
+            (gate_left_ref, w_gate.at[1, early]),
+            (gate_right_ref, w_gate.at[2, early]),
         ))
     ]
     for copy in locals_:
@@ -201,10 +289,13 @@
     run_max[...] = jnp.full_like(run_max, -jnp.inf)
     run_sum[...] = jnp.zeros_like(run_sum)
     mixed[...] = jnp.zeros_like(mixed)
+    for ring in over_y:
+        pass_on(ring)
+    start_both(gates)
+    start_both(ups)
     locals_[0].wait()
     for copy in along_z:
         copy.wait_recv()
-
     def attend(which_core, which_x):
         keys = buf.shape[2] * buf.shape[3]
 
@@ -251,37 +342,70 @@
     to_right.start()
     to_left.start()
     lines[0].start()
+    spread(
+        lambda to: remote(
+            send_ref.at[to], arrived.at[me], disp_send, disp_recv, member(to)
+        ).start()
+    )
+    row_hop.wait_recv()
+
+    def relay_row(k, carry):
+        remote(
+            row_relay.at[k], arrived.at[relay_origin], disp_send, disp_recv,
+            member(relay_target * blocks + k),
+        ).start()
+        return carry
+
+    lax.fori_loop(0, relayed, relay_row, 0)
+
     attend(core, x)
     lines[0].wait_recv()
     attend(1 - core, x)
+    for ring, right_left, lines_now in zip(over_y, over_x, over_cores):
+        far_arrived(ring)
+        start_both(right_left)
+        lines_now[0].start()
     to_right.wait_recv()
     on_right.start()
     lines[1].start()
     to_left.wait_recv()
     on_left.start()
     lines[2].start()
-    pass_on(gates)
+    gates[0].wait_recv()
+    gates[1].wait_recv()
+    gates[3].start()
     attend(core, x_left)
     attend(core, x_right)
-    on_right.wait_recv()
-    on_left.wait_recv()
-    lines[3].start()
     lines[1].wait_recv()
+    attend(1 - core, x_left)
     pass_on(ups)
-    for n in range(CHUNKS):
-        start_both(downs[n])
-    attend(1 - core, x_left)
+    start_both(downs[0])
+    start_both(downs[1])
     lines[2].wait_recv()
     attend(1 - core, x_right)
-    attend(core, x_far)
-    lines[3].wait_recv()
-    attend(1 - core, x_far)
-    attn_ref[...] = (mixed[...] / run_sum[...]).astype(attn_ref.dtype)
+
+    def activated(source, gate_now, up_now):
+        gate_proj = jnp.dot(source, gate_now, preferred_element_type=jnp.float32)
+        up_proj = jnp.dot(source, up_now, preferred_element_type=jnp.float32)
+        return (gate_proj / (1.0 + jnp.exp(-gate_proj)) * up_proj).astype(jnp.bfloat16)
+
+    def shared_part(slot):
+        value = activated(normed_ref[...], s_gate[slot], s_up[slot])
+        for n in range(CHUNKS):
+            columns = slice(n * width, (n + 1) * width)
+            product = jnp.dot(value, s_down[slot, :, columns], preferred_element_type=jnp.float32)
+            product = product.astype(jnp.bfloat16).astype(jnp.float32)
+            if slot == 0:
+                shared_sum[:, columns] = product
+            else:
+                shared_sum[:, columns] += product
+
+    for copy in locals_[1:]:
+        copy.wait()
+    shared_part(0)
 
     others = pl.ds(0, experts - 1)
     pltpu.make_async_copy(arrived.at[others], arrived.at[others], disp_recv).wait()
-    for copy in locals_[1:]:
-        copy.wait()
 
     def flatten(i, carry):
         block = arrived[pl.ds(i * 8, 8)].astype(jnp.float32).reshape(8 * capacity, model_width)
@@ -289,11 +413,6 @@
         return carry
 
     lax.fori_loop(0, experts // 8, flatten, 0)
-
-    def activated(source, gate_now, up_now):
-        gate_proj = jnp.dot(source, gate_now, preferred_element_type=jnp.float32)
-        up_proj = jnp.dot(source, up_now, preferred_element_type=jnp.float32)
-        return (gate_proj / (1.0 + jnp.exp(-gate_proj)) * up_proj).astype(jnp.bfloat16)
 
     def fill_hidden(slot):
         def tile(i, carry):
@@ -305,18 +424,36 @@
 
         lax.fori_loop(0, rows.shape[0] // TILE, tile, 0)
 
-    for slot in range(3):
-        fill_hidden(slot)
+    fill_hidden(0)
+    fill_hidden(1)
+    fill_hidden(2)
     pass_on(downs[0])
+    start_both(downs[2])
     far_arrived(gates)
     far_arrived(ups)
     fill_hidden(3)
-    shared_ring = ring_copies(group, normed_ref, whole, tokens, g_send, g_recv)
+    pass_on(downs[1])
+    start_both(downs[3])
+
+    def result_hop(n):
+        return remote(
+            out.at[n, far_blocks], result_relay.at[n],
+            relay_send.at[1 + n], relay_recv.at[1 + n], {Z: z_below},
+        )
+
+    def relay_results(n):
+        result_hop(n).wait_recv()
+
+        def step(k, carry):
+            remote(
+                result_relay.at[n, k], returned.at[n, relay_origin], ret_send.at[n], ret_recv.at[n],
+                member(relay_target * blocks + k),
+            ).start()
+            return carry
+
+        lax.fori_loop(0, relayed, step, 0)
+
     for n in range(CHUNKS):
-        if n + 1 < CHUNKS:
-            pass_on(downs[n + 1])
-        else:
-            start_both(shared_ring)
         far_arrived(downs[n])
 
         def product(i, carry, n=n):
@@ -333,63 +470,59 @@
             return carry
 
         lax.fori_loop(0, rows.shape[0] // TILE, product, 0)
-
-        def send_back(i, carry, n=n):
-            to = lax.rem(me + lax.rem(i * 13, experts), experts)
-            remote(
+        result_hop(n).start()
+        spread(
+            lambda to, n=n: remote(
                 out.at[n, to], returned.at[n, me], ret_send.at[n], ret_recv.at[n], member(to)
             ).start()
-            return carry
-
-        lax.fori_loop(1, experts, send_back, 0)
-        pltpu.make_async_copy(out.at[n, me], returned.at[n, me], own_sem.at[9 + n]).start()
-
-    pass_on(shared_ring)
-
-    def shared_part(slot):
-        value = activated(group[slot], s_gate[...], s_up[...])
-        for n in range(CHUNKS):
-            columns = slice(n * width, (n + 1) * width)
-            part[slot, :, columns] = jnp.dot(
-                value, s_down[:, columns], preferred_element_type=jnp.float32
-            ).astype(jnp.bfloat16)
-
-    top, bottom = pl.ds(0, tokens // 2), pl.ds(tokens // 2, tokens // 2)
-    part_left = remote(part.at[1], part_in.at[2], p_send.at[0], p_recv.at[0], left)
-    part_right = remote(part.at[2], part_in.at[1], p_send.at[1], p_recv.at[1], right)
-    via_right = remote(part.at[3, top], relay.at[0], p_send.at[2], p_recv.at[2], right)
-    via_left = remote(part.at[3, bottom], relay.at[1], p_send.at[3], p_recv.at[3], left)
-    on_to_right = remote(relay.at[0], part_in.at[0, top], p_send.at[4], p_recv.at[4], right)
-    on_to_left = remote(relay.at[1], part_in.at[0, bottom], p_send.at[5], p_recv.at[5], left)
-    shared_part(1)
-    part_left.start()
-    shared_part(2)
-    part_right.start()
-    far_arrived(shared_ring)
-    shared_part(3)
-    via_right.start()
-    via_left.start()
-    shared_part(0)
-    via_right.wait_recv()
-    on_to_right.start()
-    via_left.wait_recv()
-    on_to_left.start()
-    part_left.wait_recv()
-    part_right.wait_recv()
-    on_to_right.wait_recv()
-    on_to_left.wait_recv()
+        )
+        pltpu.make_async_copy(out.at[n, me], returned.at[n, me], own_sem.at[10 + n]).start()
+        if n + 2 < CHUNKS:
+            pass_on(downs[n + 2])
+        if n > 0:
+            relay_results(n - 1)
+        if n == 0:
+            for right_left, lines_now in zip(over_x, over_cores):
+                pass_on(right_left)
+                lines_now[1].start()
+                lines_now[2].start()
+        if n == 1:
+            on_right.wait_recv()
+            on_left.wait_recv()
+            lines[3].start()
+        if n == 2:
+            for right_left, lines_now in zip(over_x, over_cores):
+                far_arrived(right_left)
+                lines_now[3].start()
+    attend(core, x_far)
+    relay_results(CHUNKS - 1)
+    lines[3].wait_recv()
+    attend(1 - core, x_far)
+    head_rows = attn_ref.shape[0]
+    size = 64
+    for pair in range(attn_ref.shape[1] // 128):
+        heads = []
+        for head in (2 * pair, 2 * pair + 1):
+            here = slice(head * head_rows, (head + 1) * head_rows)
+            heads.append((mixed[here, :] / run_sum[here, :])[:, size:])
+        attn_ref[:, pair * 128 : (pair + 1) * 128] = jnp.concatenate(heads, axis=1).astype(
+            attn_ref.dtype
+        )
+    for lines_now in over_cores:
+        for copy in lines_now:
+            copy.wait_recv()
+    for slot in range(1, 4):
+        shared_part(slot)
 
     for n in range(CHUNKS):
         pltpu.make_async_copy(
             returned.at[n, others], returned.at[n, others], ret_recv.at[n]
         ).wait()
-        pltpu.make_async_copy(out.at[n, me], returned.at[n, me], own_sem.at[9 + n]).wait()
+        pltpu.make_async_copy(out.at[n, me], returned.at[n, me], own_sem.at[10 + n]).wait()
         columns = slice(n * width, (n + 1) * width)
         results = returned[n].astype(jnp.float32).reshape(experts * capacity, width)
         results = results.astype(jnp.bfloat16)
-        total = part[0, :, columns].astype(jnp.float32)
-        for slot in range(3):
-            total = total + part_in[slot, :, columns].astype(jnp.float32)
+        total = shared_sum[:, columns]
         routed = None
         for k in range(pick_ref.shape[0]):
             picked = jnp.dot(pick_ref[k], results, preferred_element_type=jnp.float32)
@@ -397,19 +530,19 @@
             routed = term if routed is None else routed + term
         moe_ref[:, columns] = (routed + total).astype(moe_ref.dtype)
 
-    for ring in [gates, ups, shared_ring] + downs:
+    for ring in [gates, ups] + downs + over_y + over_x + over_cores:
         for copy in ring:
             copy.wait_send()
-    for copy in along_z + [to_right, to_left, on_right, on_left] + lines:
+    for copy in along_z + [to_right, to_left, on_right, on_left, row_hop] + lines:
         copy.wait_send()
-    for copy in (part_left, part_right, via_right, via_left, on_to_right, on_to_left):
-        copy.wait_send()
+    for n in range(CHUNKS):
+        result_hop(n).wait_send()
     pltpu.make_async_copy(send_ref.at[others], arrived.at[others], disp_send).wait()
     for n in range(CHUNKS):
         pltpu.make_async_copy(out.at[n, others], returned.at[n, others], ret_send.at[n]).wait()
 
 
-def run_layer(q_rows, key_value, send, normed, picks, scales, expert_weights, shared_weights):
+def run_layer(q_rows, key_value, send, normed, picks, scales, early, expert_weights, shared_weights):
     query_count = q_rows.shape[0]
     tokens = key_value.shape[0]
     z_size, x_size, cores = (lax.axis_size(name) for name in EP)
@@ -424,10 +557,10 @@
     return pl.pallas_call(
         layer_kernel,
         out_shape=[
-            jax.ShapeDtypeStruct((query_count, 128), bf16),
+            jax.ShapeDtypeStruct((tokens, query_count // tokens * 64), bf16),
             jax.ShapeDtypeStruct(normed.shape, bf16),
         ],
-        in_specs=[vmem, vmem, anywhere, vmem, vmem, vmem] + [anywhere] * 6,
+        in_specs=[vmem, vmem, anywhere, vmem, vmem, vmem] + [anywhere] * 8,
         out_specs=[vmem, vmem],
         scratch_shapes=[
             pltpu.VMEM((cores, x_size, z_size, tokens, 128), bf16),
@@ -437,18 +570,17 @@
             pltpu.VMEM((4, depth, units), bf16),
             pltpu.VMEM((4, depth, units), bf16),
             pltpu.VMEM((4, units, depth), bf16),
-            pltpu.VMEM((depth, units), bf16),
-            pltpu.VMEM((depth, units), bf16),
-            pltpu.VMEM((units, depth), bf16),
+            pltpu.VMEM((4, depth, units), bf16),
+            pltpu.VMEM((4, depth, units), bf16),
+            pltpu.VMEM((4, units, depth), bf16),
             pltpu.VMEM((experts, capacity, model_width), bf16),
             pltpu.VMEM((rows, model_width), bf16),
             pltpu.VMEM((rows, 4 * units), bf16),
             pltpu.VMEM((CHUNKS, experts, capacity, width), bf16),
             pltpu.VMEM((CHUNKS, experts, capacity, width), bf16),
-            pltpu.VMEM((4, own, model_width), bf16),
-            pltpu.VMEM((4, own, model_width), bf16),
-            pltpu.VMEM((3, own, model_width), bf16),
-            pltpu.VMEM((2, own // 2, model_width), bf16),
+            pltpu.VMEM((own, model_width), f32),
+            pltpu.VMEM((x_size * cores // 2, capacity, model_width), bf16),
+            pltpu.VMEM((CHUNKS, x_size * cores // 2, capacity, width), bf16),
             dma((z_size,)), dma((z_size,)),
             dma((4,)), dma((4,)),
             dma((4,)), dma((4,)),
@@ -456,9 +588,11 @@
             dma((CHUNKS, 4)), dma((CHUNKS, 4)),
             dma, dma,
             dma((CHUNKS,)), dma((CHUNKS,)),
-            dma((4,)), dma((4,)),
-            dma((6,)), dma((6,)),
-            dma((9 + CHUNKS,)),
+            dma((3, 4)), dma((3, 4)),
+            dma((3, 4)), dma((3, 4)),
+            dma((3, 4)), dma((3, 4)),
+            dma((1 + CHUNKS,)), dma((1 + CHUNKS,)),
+            dma((10 + CHUNKS,)),
         ],
         compiler_params=pltpu.CompilerParams(
             collective_id=0, has_side_effects=True, vmem_limit_bytes=60 * 1024 * 1024
@@ -467,7 +601,7 @@
             flops=60 * query_count * keys * 128 // 2, bytes_accessed=2 * keys * 256, transcendentals=0
         ),
         name="layer",
-    )(q_rows, key_value, send, normed, picks, scales, *expert_weights, *shared_weights)
+    )(q_rows, key_value, send, normed, picks, scales, *early, *expert_weights, *shared_weights)
 
 
 def dispatch(moe_tokens, norm_gain, routes, route_weights):
@@ -512,6 +646,8 @@
     shared_up,
     shared_down,
 ):
+    first_half = expert_gate[0, : expert_gate.shape[1] // 2]
+    early = (lax.ppermute(first_half, "tp", ring(1)), lax.ppermute(first_half, "tp", ring(3)))
     dispatched = dispatch(moe_tokens, norm_gain, routes, route_weights)
     row_count = query_rows.shape[0]
     size = query_gain.shape[0]
@@ -525,11 +661,11 @@
         q_rot.reshape(heads * row_count, 128),
         k_rot + values,
         *dispatched,
+        early,
         (expert_gate[0], expert_up[0], expert_down[0]),
         (shared_gate, shared_up, shared_down),
     )
-    attn_out = attn[:, size:].reshape(heads, row_count, size).transpose(1, 0, 2)
-    return (attn_out.reshape(row_count, heads * size), moe_out)
+    return (attn, moe_out)
 
 
 def solution(mesh):

time: 185 us -> 180 us (0.973)
  Pallas kernels: 163 us -> 156 us
  starting transfers between devices: 0 us -> 2.24 us
    pallas_call x1, Pallas kernels: 163 us -> 156 us  [run_layer(): pl.pallas_call(layer_kernel, out_shape=[jax.ShapeDtypeStruct((tokens, que...]
    ppermute x0 -> x2, starting transfers between devices: none -> 2.24 us  [the longest x1 2.23 us: body(): lax.ppermute(first_half, 'tp', ring(3))]
  transfers between devices with their start and end apart: 0 -> 2, of which waited for: 0 -> 0; matrix products, arithmetic and copies ran while one was open for 0% -> 8% of each run, Pallas kernels for 0% -> 0%
where the time goes in v4:
time: 180 us; the launch traced here: 179 us
  Pallas kernels  156 us (87%)
  local copies, waits for them, and re-layouts  10.3 us (6%)
  matrix products  5.17 us (3%)
  other arithmetic  4.56 us (3%)
  starting transfers between devices  2.24 us (1%)
    pallas_call x1, Pallas kernels, run_layer(): pl.pallas_call(layer_kernel, out_shape=[jax.ShapeDtypeStruct((tokens, que...  156 us
  transfers between devices with their start and end apart: 2, of which 0 were waited for; matrix products, arithmetic and copies ran while one was open for 8% of the time, Pallas kernels for 0%

profile of v4, /device:TPU:8, one launch (start us, length us, event | category | flops | bytes accessed | tf_op | source)
XLA Modules:
  0.0 179.2 jit_solution(17900455987445974050)
XLA Ops:
  0.6 1.1 slice_bitcast_fusion
  1.8 2.2 %collective-permute-start.1 = (bf16[1024,256]{1,0:T(8,128)(2,1)S(1)}, bf16[1024,256]{1,0:T(8,128)(2,1)S(1)}, u32[]{:S(2)}, u32[]{:S(2)}) collective-permute-start(bf16[1024,256]{1,0:T(8,128)(2,1)S(1)} %slice_bitcast_fusion), channel_id=1, source_target_pairs={{0,3},{1,0},{2,1},{3,2},{4,7},{5,4},{6,5},{7,6},{8,11},{9,8},{10,9... | collective-permute-start | bytes 1572872 | tf_op jit(solution)/shard_map/ppermute | solution.py:650
  4.0 0.7 constant_dynamic-slice_fusion
  4.7 0.1 convert_reduce_fusion.1
  4.9 0.8 reshape.644
  5.7 0.7 pad.13
  6.3 0.7 pad.15
  7.0 0.7 reshape.647
  7.7 1.2 fusion.16
  9.0 0.8 dynamic-slice_reduce_fusion
  9.8 0.1 rev.6
  9.8 0.1 reshape.645
  10.0 0.1 rev.7
  10.0 0.1 reshape.648
  10.1 1.1 multiply_reduce_fusion.1
  11.2 0.1 broadcast_add_fusion
  11.3 0.3 multiply_reduce_fusion
  11.6 0.6 fusion.34
  12.2 0.3 fusion.6
  12.5 0.8 copy.25
  13.4 0.1 iota_compare_fusion.2
  13.5 0.7 add_convert_fusion.pick_ref
  14.2 0.2 fusion.18.normed_ref
  14.4 2.0 %fusion.send_ref = bf16[64,8,2048]{2,1,0:T(8,128)(2,1)} fusion(bf16[128,2048]{1,0:T(8,128)(2,1)S(1)} %fusion.18.normed_ref, s32[128]{0:T(128)S(1)} %get-tuple-element.9, s32[128]{0:T(128)S(1)} %get-tuple-element.8), kind=kOutput, calls=%fused_computation.1 | convolution fusion | flops 269680640 | bytes 2622464 | tf_op jit(solution)/shard_map/dot_general | solution.py:625
  16.5 0.6 fusion.15
  17.1 0.7 multiply_bitcast_fusion
  17.8 0.8 fusion.14.kv_ref
  18.7 0.9 broadcast_in_dim.59.scale_ref
  19.5 0.1 copy-done.7
  19.7 156.1 %layer.1 = (bf16[256,256]{1,0:T(8,128)(2,1)}, bf16[128,2048]{1,0:T(8,128)(2,1)}) custom-call(bf16[1024,128]{1,0:T(8,128)(2,1)} %bitcast.94, bf16[256,128]{1,0:T(8,128)(2,1)} %fusion.14.kv_ref, bf16[64,8,2048]{2,1,0:T(8,128)(2,1)} %fusion.send_ref, bf16[128,2048]{1,0:T(8,128)(2,1)} %copy-done.1, bf16[2,128,512]{2,1,0:T(8,128)(2,1)} %add_convert_fusion.pick_ref, ...), custom_call_target="tpu_custom_call" | custom-call | flops 64424509440 | bytes 8388608 | tf_op jit(solution)/shard_map/layer/pallas_call | solution.py:557
  175.8 1.6 copy.34
  177.4 1.9 %copy.35 = bf16[128,2048]{1,0:T(8,128)(2,1)} copy(bf16[128,2048]{1,0:T(8,128)(2,1)} %get-tuple-element.29) | data formatting | bytes 1048576
  (33 shorter events, 0.1 us)
Async XLA Ops:
  0.6 10.7 %copy-start = (bf16[256,256]{1,0:T(8,128)(2,1)S(1)}, bf16[256,256]{1,0:T(8,128)(2,1)}, u32[]{:S(2)}) copy-start(bf16[256,256]{1,0:T(8,128)(2,1)} %param.15) | copy-start | bytes 393220
  1.8 16.9 %collective-permute-start.1 = (bf16[1024,256]{1,0:T(8,128)(2,1)S(1)}, bf16[1024,256]{1,0:T(8,128)(2,1)S(1)}, u32[]{:S(2)}, u32[]{:S(2)}) collective-permute-start(bf16[1024,256]{1,0:T(8,128)(2,1)S(1)} %slice_bitcast_fusion), channel_id=1, source_target_pairs={{0,3},{1,0},{2,1},{3,2},{4,7},{5,4},{6,5},{7,6},{8,11},{9,8},{10,9... | collective-permute-start | bytes 1572872 | tf_op jit(solution)/shard_map/ppermute | solution.py:650
  4.0 14.7 %collective-permute-start = (bf16[1024,256]{1,0:T(8,128)(2,1)S(1)}, bf16[1024,256]{1,0:T(8,128)(2,1)S(1)}, u32[]{:S(2)}, u32[]{:S(2)}) collective-permute-start(bf16[1024,256]{1,0:T(8,128)(2,1)S(1)} %slice_bitcast_fusion), channel_id=1, source_target_pairs={{0,1},{1,2},{2,3},{3,0},{4,5},{5,6},{6,7},{7,4},{8,9},{9,10},{10,1... | collective-permute-start | bytes 1572872 | tf_op jit(solution)/shard_map/ppermute | solution.py:650
  9.0 5.3 %copy-start.2 = (bf16[128,2048]{1,0:T(8,128)(2,1)S(1)}, bf16[128,2048]{1,0:T(8,128)(2,1)}, u32[]{:S(2)}) copy-start(bf16[128,2048]{1,0:T(8,128)(2,1)} %param.20) | copy-start | bytes 1572868
  9.0 5.3 %copy-start.5 = (f32[2048]{0:T(1024)S(1)}, f32[2048]{0:T(1024)}, u32[]{:S(2)}) copy-start(f32[2048]{0:T(1024)} %param.21) | copy-start | bytes 24580
  13.4 3.1 %copy-start.3 = (bf16[256,64]{0,1:T(8,128)(2,1)S(1)}, bf16[256,64]{0,1:T(8,128)(2,1)}, u32[]{:S(2)}) copy-start(bf16[256,64]{0,1:T(8,128)(2,1)} %param.16) | copy-start | bytes 98308
  14.2 3.6 %copy-start.4 = (bf16[256,64]{0,1:T(8,128)(2,1)S(1)}, bf16[256,64]{0,1:T(8,128)(2,1)}, u32[]{:S(2)}) copy-start(bf16[256,64]{0,1:T(8,128)(2,1)} %param.17) | copy-start | bytes 98308
  14.4 5.1 %copy-start.1 = (bf16[128,2048]{1,0:T(8,128)(2,1)}, bf16[128,2048]{1,0:T(8,128)(2,1)S(1)}, u32[]{:S(2)}) copy-start(bf16[128,2048]{1,0:T(8,128)(2,1)S(1)} %fusion.18.normed_ref) | copy-start | bytes 1572868
  18.6 0.9 copy-start.6
  18.7 1.0 copy-start.7

commit v5 on v4

--- a/solution.py
+++ b/solution.py
@@ -380,7 +380,6 @@
     attend(1 - core, x_left)
     pass_on(ups)
     start_both(downs[0])
-    start_both(downs[1])
     lines[2].wait_recv()
     attend(1 - core, x_right)
 
@@ -428,12 +427,10 @@
     fill_hidden(1)
     fill_hidden(2)
     pass_on(downs[0])
-    start_both(downs[2])
+    start_both(downs[1])
     far_arrived(gates)
     far_arrived(ups)
     fill_hidden(3)
-    pass_on(downs[1])
-    start_both(downs[3])
 
     def result_hop(n):
         return remote(
@@ -477,8 +474,10 @@
             ).start()
         )
         pltpu.make_async_copy(out.at[n, me], returned.at[n, me], own_sem.at[10 + n]).start()
+        if n + 1 < CHUNKS:
+            pass_on(downs[n + 1])
         if n + 2 < CHUNKS:
-            pass_on(downs[n + 2])
+            start_both(downs[n + 2])
         if n > 0:
             relay_results(n - 1)
         if n == 0:

time: 180 us -> 177 us (0.983); the launches traced: 179 us -> 174 us
  Pallas kernels: 156 us -> 151 us
    pallas_call x1, Pallas kernels: 156 us -> 151 us  [run_layer(): pl.pallas_call(layer_kernel, out_shape=[jax.ShapeDtypeStruct((tokens, que...]
where the time goes in v5:
time: 177 us; the launch traced here: 174 us
  Pallas kernels  151 us (85%)
  local copies, waits for them, and re-layouts  10.3 us (6%)
  matrix products  5.17 us (3%)
  other arithmetic  4.56 us (3%)
  starting transfers between devices  2.24 us (1%)
    pallas_call x1, Pallas kernels, run_layer(): pl.pallas_call(layer_kernel, out_shape=[jax.ShapeDtypeStruct((tokens, que...  151 us
    unnamed x18, local copies, waits for them, and re-layouts  3.6 us
  transfers between devices with their start and end apart: 2, of which 0 were waited for; matrix products, arithmetic and copies ran while one was open for 8% of the time, Pallas kernels for 0%

profile of v5, /device:TPU:8, one launch (start us, length us, event | category | flops | bytes accessed | tf_op | source)
XLA Modules:
  0.0 173.9 jit_solution(369934174666368401)
XLA Ops:
  0.6 1.1 slice_bitcast_fusion
  1.8 2.2 %collective-permute-start.1 = (bf16[1024,256]{1,0:T(8,128)(2,1)S(1)}, bf16[1024,256]{1,0:T(8,128)(2,1)S(1)}, u32[]{:S(2)}, u32[]{:S(2)}) collective-permute-start(bf16[1024,256]{1,0:T(8,128)(2,1)S(1)} %slice_bitcast_fusion), channel_id=1, source_target_pairs={{0,3},{1,0},{2,1},{3,2},{4,7},{5,4},{6,5},{7,6},{8,11},{9,8},{10,9... | collective-permute-start | bytes 1572872 | tf_op jit(solution)/shard_map/ppermute | solution.py:649
  4.0 0.7 constant_dynamic-slice_fusion
  4.7 0.1 convert_reduce_fusion.1
  4.9 0.8 reshape.644
  5.7 0.7 pad.13
  6.3 0.7 pad.15
  7.0 0.7 reshape.647
  7.7 1.2 fusion.16
  9.0 0.8 dynamic-slice_reduce_fusion
  9.8 0.1 rev.6
  9.8 0.1 reshape.645
  10.0 0.1 rev.7
  10.0 0.1 reshape.648
  10.1 1.1 multiply_reduce_fusion.1
  11.2 0.1 broadcast_add_fusion
  11.3 0.3 multiply_reduce_fusion
  11.6 0.6 fusion.34
  12.2 0.3 fusion.6
  12.5 0.8 copy.25
  13.4 0.1 iota_compare_fusion.2
  13.5 0.7 add_convert_fusion.pick_ref
  14.2 0.2 fusion.18.normed_ref
  14.4 2.0 %fusion.send_ref = bf16[64,8,2048]{2,1,0:T(8,128)(2,1)} fusion(bf16[128,2048]{1,0:T(8,128)(2,1)S(1)} %fusion.18.normed_ref, s32[128]{0:T(128)S(1)} %get-tuple-element.9, s32[128]{0:T(128)S(1)} %get-tuple-element.8), kind=kOutput, calls=%fused_computation.1 | convolution fusion | flops 269680640 | bytes 2622464 | tf_op jit(solution)/shard_map/dot_general | solution.py:624
  16.5 0.6 fusion.15
  17.1 0.7 multiply_bitcast_fusion
  17.8 0.8 fusion.14.kv_ref
  18.7 0.9 broadcast_in_dim.59.scale_ref
  19.5 0.1 copy-done.7
  19.7 150.8 %layer.1 = (bf16[256,256]{1,0:T(8,128)(2,1)}, bf16[128,2048]{1,0:T(8,128)(2,1)}) custom-call(bf16[1024,128]{1,0:T(8,128)(2,1)} %bitcast.94, bf16[256,128]{1,0:T(8,128)(2,1)} %fusion.14.kv_ref, bf16[64,8,2048]{2,1,0:T(8,128)(2,1)} %fusion.send_ref, bf16[128,2048]{1,0:T(8,128)(2,1)} %copy-done.1, bf16[2,128,512]{2,1,0:T(8,128)(2,1)} %add_convert_fusion.pick_ref, ...), custom_call_target="tpu_custom_call" | custom-call | flops 64424509440 | bytes 8388608 | tf_op jit(solution)/shard_map/layer/pallas_call | solution.py:556
  170.4 1.6 copy.34
  172.0 1.9 %copy.35 = bf16[128,2048]{1,0:T(8,128)(2,1)} copy(bf16[128,2048]{1,0:T(8,128)(2,1)} %get-tuple-element.29) | data formatting | bytes 1048576
  (33 shorter events, 0.1 us)
Async XLA Ops:
  0.6 10.7 %copy-start = (bf16[256,256]{1,0:T(8,128)(2,1)S(1)}, bf16[256,256]{1,0:T(8,128)(2,1)}, u32[]{:S(2)}) copy-start(bf16[256,256]{1,0:T(8,128)(2,1)} %param.15) | copy-start | bytes 393220
  1.8 16.9 %collective-permute-start.1 = (bf16[1024,256]{1,0:T(8,128)(2,1)S(1)}, bf16[1024,256]{1,0:T(8,128)(2,1)S(1)}, u32[]{:S(2)}, u32[]{:S(2)}) collective-permute-start(bf16[1024,256]{1,0:T(8,128)(2,1)S(1)} %slice_bitcast_fusion), channel_id=1, source_target_pairs={{0,3},{1,0},{2,1},{3,2},{4,7},{5,4},{6,5},{7,6},{8,11},{9,8},{10,9... | collective-permute-start | bytes 1572872 | tf_op jit(solution)/shard_map/ppermute | solution.py:649
  4.0 14.7 %collective-permute-start = (bf16[1024,256]{1,0:T(8,128)(2,1)S(1)}, bf16[1024,256]{1,0:T(8,128)(2,1)S(1)}, u32[]{:S(2)}, u32[]{:S(2)}) collective-permute-start(bf16[1024,256]{1,0:T(8,128)(2,1)S(1)} %slice_bitcast_fusion), channel_id=1, source_target_pairs={{0,1},{1,2},{2,3},{3,0},{4,5},{5,6},{6,7},{7,4},{8,9},{9,10},{10,1... | collective-permute-start | bytes 1572872 | tf_op jit(solution)/shard_map/ppermute | solution.py:649
  9.0 5.3 %copy-start.2 = (bf16[128,2048]{1,0:T(8,128)(2,1)S(1)}, bf16[128,2048]{1,0:T(8,128)(2,1)}, u32[]{:S(2)}) copy-start(bf16[128,2048]{1,0:T(8,128)(2,1)} %param.20) | copy-start | bytes 1572868
  9.0 5.3 %copy-start.5 = (f32[2048]{0:T(1024)S(1)}, f32[2048]{0:T(1024)}, u32[]{:S(2)}) copy-start(f32[2048]{0:T(1024)} %param.21) | copy-start | bytes 24580
  13.4 3.1 %copy-start.3 = (bf16[256,64]{0,1:T(8,128)(2,1)S(1)}, bf16[256,64]{0,1:T(8,128)(2,1)}, u32[]{:S(2)}) copy-start(bf16[256,64]{0,1:T(8,128)(2,1)} %param.16) | copy-start | bytes 98308
  14.2 3.6 %copy-start.4 = (bf16[256,64]{0,1:T(8,128)(2,1)S(1)}, bf16[256,64]{0,1:T(8,128)(2,1)}, u32[]{:S(2)}) copy-start(bf16[256,64]{0,1:T(8,128)(2,1)} %param.17) | copy-start | bytes 98308
  14.4 5.1 %copy-start.1 = (bf16[128,2048]{1,0:T(8,128)(2,1)}, bf16[128,2048]{1,0:T(8,128)(2,1)S(1)}, u32[]{:S(2)}) copy-start(bf16[128,2048]{1,0:T(8,128)(2,1)S(1)} %fusion.18.normed_ref) | copy-start | bytes 1572868
  18.6 0.9 copy-start.6
  18.7 1.0 copy-start.7
